TPU v7x, 256 devices: a whole 4x4x8 slice. The times are simulated.
256 devices in a mesh: ep: 128 (over z, y, x), tp: 2 (over core).
Axes of the slice: x: 4, y: 4, z: 8, core: 2. Of those that a mesh axis runs over, the one named last changes fastest.
Arguments:
- tokens: bfloat16 [2048, 2048], P('ep'), may hold values from -6 to 6
- lengths: int32 [2048], P('ep'), may hold values from 1 to 1024, as said below
- attn_gain: float32 [2048], replicated, may hold values from 0.1 to 1.9
- w_query: bfloat16 [2048, 1024], P(None, 'tp'), may hold values from -0.125 to 0.125
- w_key: bfloat16 [2048, 128], P(None, 'tp'), may hold values from -0.125 to 0.125
- w_value: bfloat16 [2048, 128], P(None, 'tp'), may hold values from -0.125 to 0.125
- head_bias: float32 [16], P('tp'), may hold values from -7 to -2
- key_cache: bfloat16 [2048, 2, 64, 1024], P('ep', 'tp'), may hold values from -6 to 6
- value_cache: bfloat16 [2048, 2, 64, 1024], P('ep', 'tp'), may hold values from -6 to 6
- w_attn_out: bfloat16 [1024, 2048], P('tp'), may hold values from -0.1875 to 0.1875
- ffn_gain: float32 [2048], replicated, may hold values from 0.1 to 1.9
- w_router: bfloat16 [2048, 128], replicated, may hold values from -0.125 to 0.125
- routes: int32 [2048, 6], P('ep'), may hold values from 0 to 127, all different within a row; in each aligned block of 16 rows (0 to 15, 16 to 31, ...) at most 2 rows name the same one
- w_dense_gate: bfloat16 [2048, 512], P('ep', 'tp'), may hold values from -0.125 to 0.125
- w_dense_up: bfloat16 [2048, 512], P('ep', 'tp'), may hold values from -0.125 to 0.125
- w_dense_down: bfloat16 [512, 2048], P('tp', 'ep'), may hold values from -0.25 to 0.25
- dense_mix: float32 [2048], replicated, may hold values from -0.125 to 0.125
- w_expert_gate: bfloat16 [128, 2048, 512], P('ep', None, 'tp'), may hold values from -0.125 to 0.125
- w_expert_up: bfloat16 [128, 2048, 512], P('ep', None, 'tp'), may hold values from -0.125 to 0.125
- w_expert_down: bfloat16 [128, 512, 2048], P('ep', 'tp'), may hold values from -0.25 to 0.25
Outputs:
- layer_out: bfloat16 [2048, 2048], P('ep', 'tp')
- new_keys: bfloat16 [2048, 128], P('ep', 'tp')
- new_values: bfloat16 [2048, 128], P('ep', 'tp')
Inputs may be any that keep to these rules, and one draw needn't show every extreme that they name: `lengths`: every sequence holds between 1 and 1024 cached positions; in every draw some sequence holds exactly 1024. `routes`: each token names 6 different experts. Among the rows of one device no expert is named by more than 2 rows.
All inputs are finite; a program needn't handle non-finite values.
Results may differ from a plain program's by a relative error of at most 0.014.
Values may be sent and summed in bfloat16 or wider, within the bound.
A program may use at most 64 MiB of HBM per device.

v0:
```python
import jax
import jax.numpy as jnp
from jax import lax
from jax.sharding import Mesh
from jax.sharding import PartitionSpec as P

EP = ("ep_0", "ep_1", "ep_2")


def cut_along(x, dim, size):
    shape = x.shape
    parts = x.reshape(*shape[:dim], size, shape[dim] // size, *shape[dim + 1 :])
    return jnp.moveaxis(parts, dim, 0)


def sum_at_owner(x, axis, dim):
    size = lax.axis_size(axis)
    parts = lax.all_to_all(cut_along(x, dim, size), axis, 0, 0, tiled=True)
    return jnp.sum(parts.astype(jnp.float32), axis=0)


def from_everyone(x, axis):
    copies = jnp.broadcast_to(x, (lax.axis_size(axis), *x.shape))
    return lax.all_to_all(copies, axis, split_axis=0, concat_axis=0, tiled=True)


def of_everyone(x, axis):
    return from_everyone(x, axis).astype(jnp.float32).sum(axis=0)


def laid_out(parts, dim):
    shape = list(parts.shape[1:])
    shape[dim] *= parts.shape[0]
    return jnp.moveaxis(parts, 0, dim).reshape(shape)


def collect(x, axis, dim):
    return laid_out(from_everyone(x, axis), dim)


def grouped_exchange(x, axis, split_dim, concat_dim, work, item_dim, out_dim):
    items = jax.tree.leaves(x)[0].shape[item_dim]
    count = 2 if items % 2 == 0 else 1
    finished = []
    for k in range(count):
        group = jax.tree.map(
            lambda a: lax.slice_in_dim(
                a, k * (items // count), (k + 1) * (items // count), axis=item_dim
            ),
            x,
        )
        finished.append(
            work(
                lax.all_to_all(
                    group, axis, split_axis=split_dim, concat_axis=concat_dim, tiled=True
                )
            )
        )
    return jax.tree.map(lambda *parts: jnp.concatenate(parts, axis=out_dim), *finished)


def sent_together(arrays, axis, dim, along):
    widths = [a.shape[along] for a in arrays]
    both = jnp.concatenate(arrays, axis=along)
    out = lax.all_gather(both, axis, axis=dim, tiled=True)
    return tuple(jnp.split(out, [sum(widths[:k]) for k in range(1, len(widths))], axis=along))


def gather_axes(x, axes, dim):
    for axis in reversed(axes):
        x = lax.all_gather(x, axis, axis=dim, tiled=True)
    return x


def rms_scale(values, gain):
    wide = values.astype(jnp.float32)
    return wide * lax.rsqrt(jnp.mean(wide * wide, axis=-1, keepdims=True) + 1e-06) * gain


def stick_read(queries, lengths, head_bias, key_cache, value_cache):
    seq_count, local_kv, head_dim, cache_len = key_cache.shape
    group_size = head_bias.shape[0] // local_kv
    grouped = queries.reshape(seq_count, local_kv, group_size, head_dim)
    head_shift = head_bias.reshape(1, local_kv, group_size, 1)
    span_len = min(512, cache_len)
    block_count = (jnp.max(lengths) + span_len - 1) // span_len
    span_index = lax.iota(jnp.int32, span_len)
    after_mask = (span_index[:, None] > span_index[None, :]).astype(jnp.float32)

    def visit(visit_index, carry):
        totals, log_later = carry
        first = (block_count - 1 - visit_index) * span_len
        key_block = lax.dynamic_slice_in_dim(key_cache, first, span_len, 3)
        value_block = lax.dynamic_slice_in_dim(value_cache, first, span_len, 3)
        scores = (
            jnp.einsum("skgd,skdc->skgc", grouped, key_block, preferred_element_type=jnp.float32)
            * head_dim ** (-0.5)
            + head_shift
        )
        positions = first + span_index
        visible = (positions[None, :] < lengths[:, None])[:, None, None, :]
        log_keep = jnp.where(visible, jax.nn.log_sigmoid(-scores), 0.0)
        log_after = jnp.einsum("skgj,jc->skgc", log_keep, after_mask) + log_later[..., None]
        weights = jnp.where(visible, jnp.exp(jax.nn.log_sigmoid(scores) + log_after), 0.0).astype(
            jnp.bfloat16
        )
        totals = totals + jnp.einsum(
            "skgc,skdc->skgd", weights, value_block, preferred_element_type=jnp.float32
        )
        return (totals, log_later + jnp.sum(log_keep, axis=3))

    start_totals = jnp.zeros((seq_count, local_kv, group_size, head_dim), jnp.float32)
    start_later = jnp.zeros((seq_count, local_kv, group_size), jnp.float32)
    totals, unused_later = lax.fori_loop(0, block_count, visit, (start_totals, start_later))
    return totals.reshape(seq_count, -1).astype(jnp.bfloat16)


def expert_math(inputs, w_expert_gate, w_expert_up, w_expert_down):
    gate_rows = jnp.einsum(
        "njcd,jdf->njcf", inputs, w_expert_gate, preferred_element_type=jnp.float32
    )
    up_rows = jnp.einsum("njcd,jdf->njcf", inputs, w_expert_up, preferred_element_type=jnp.float32)
    hidden = (jax.nn.silu(gate_rows) * up_rows).astype(jnp.bfloat16)
    partial_value = jnp.einsum(
        "njcf,jfd->njcd", hidden, w_expert_down, preferred_element_type=jnp.float32
    ).astype(jnp.bfloat16)
    return sum_at_owner(partial_value, "tp", 3).astype(jnp.bfloat16)


def shards(
    tokens,
    lengths,
    attn_gain,
    w_query,
    w_key,
    w_value,
    head_bias,
    key_cache,
    value_cache,
    w_attn_out,
    ffn_gain,
    w_router,
    routes,
    w_dense_gate,
    w_dense_up,
    w_dense_down,
    dense_mix,
    w_expert_gate,
    w_expert_up,
    w_expert_down,
):
    seq_count, model_width = tokens.shape
    normed = rms_scale(tokens, attn_gain).astype(jnp.bfloat16)
    new_keys = jnp.dot(normed, w_key, preferred_element_type=jnp.float32).astype(jnp.bfloat16)
    new_values = jnp.dot(normed, w_value, preferred_element_type=jnp.float32).astype(jnp.bfloat16)
    queries = jnp.dot(normed, w_query, preferred_element_type=jnp.float32).astype(jnp.bfloat16)
    heads_out = stick_read(queries, lengths, head_bias, key_cache, value_cache)
    attn_partial = jnp.dot(heads_out, w_attn_out, preferred_element_type=jnp.float32).astype(
        jnp.bfloat16
    )
    attn = of_everyone(attn_partial, "tp").astype(jnp.float32)
    residual = (tokens.astype(jnp.float32) + attn).astype(jnp.bfloat16)
    normed2 = rms_scale(residual, ffn_gain).astype(jnp.bfloat16)
    expert_total = w_router.shape[1]
    top_count = routes.shape[1]
    probs = jax.nn.sigmoid(jnp.dot(normed2, w_router, preferred_element_type=jnp.float32))
    hits = routes[:, :, None] == lax.iota(jnp.int32, expert_total)[None, None, :]
    picked = jnp.sum(jnp.where(hits, probs[:, None, :], 0.0), axis=-1)
    gates = picked / jnp.sum(picked, axis=-1, keepdims=True) * 2.5
    capacity = max(2, 2 * seq_count * top_count // expert_total)
    slot_total = expert_total * capacity
    flat_routes = routes.reshape(-1)
    route_count = flat_routes.shape[0]
    matching = flat_routes[:, None] == flat_routes[None, :]
    earlier = lax.iota(jnp.int32, route_count)[:, None] > lax.iota(jnp.int32, route_count)[None, :]
    slot_rank = jnp.sum(jnp.logical_and(matching, earlier).astype(jnp.int32), axis=1)
    target = flat_routes * capacity + slot_rank
    one_hot = (target[:, None] == lax.iota(jnp.int32, slot_total)[None, :]).astype(jnp.bfloat16)
    dispatch = jnp.sum(one_hot.reshape(seq_count, top_count, slot_total), axis=1)
    send_rows = jnp.einsum(
        "sr,sd->rd", dispatch, normed2, preferred_element_type=jnp.float32
    ).astype(jnp.bfloat16)
    send_rows = send_rows.reshape(expert_total, capacity, model_width)
    local_experts = w_expert_gate.shape[0]
    core_count = lax.axis_size("tp")
    half_cap = capacity // core_count
    own_slots = lax.dynamic_slice_in_dim(send_rows, lax.axis_index("tp") * half_cap, half_cap, 1)

    def run_halves(received):
        source_count = received.shape[0] // local_experts
        item_count = received.shape[1]
        both = collect(received, "tp", 0)
        inputs = both.reshape(core_count * source_count, local_experts, item_count, model_width)
        summed = expert_math(inputs, w_expert_gate, w_expert_up, w_expert_down)
        summed = summed.reshape(
            core_count, source_count * local_experts, item_count, summed.shape[3]
        )
        return lax.all_to_all(summed, EP, split_axis=1, concat_axis=1, tiled=True)

    returned = grouped_exchange(own_slots, EP, 0, 0, run_halves, 1, 2)
    half_width = returned.shape[3]
    split_target = (
        slot_rank // half_cap * (expert_total * half_cap)
        + flat_routes * half_cap
        + slot_rank % half_cap
    )
    route_rows = returned.reshape(-1, half_width)[split_target]
    route_rows = route_rows.reshape(seq_count, top_count, half_width)
    routed = jnp.sum(gates[:, :, None] * route_rows.astype(jnp.float32), axis=1)
    portions = sent_together((w_dense_gate, w_dense_up), EP, 0, 1)
    gate_sum = jnp.dot(normed2, portions[0], preferred_element_type=jnp.float32)
    up_sum = jnp.dot(normed2, portions[1], preferred_element_type=jnp.float32)
    dense_hidden = (jax.nn.silu(gate_sum) * up_sum).astype(jnp.bfloat16)
    dense_partial = jnp.dot(
        dense_hidden, gather_axes(w_dense_down, EP, 1), preferred_element_type=jnp.float32
    ).astype(jnp.bfloat16)
    dense = sum_at_owner(dense_partial, "tp", 1)
    mix_gate = jax.nn.sigmoid(jnp.sum(normed2.astype(jnp.float32) * dense_mix, axis=-1))
    offset = lax.axis_index("tp") * half_width
    residual_half = lax.dynamic_slice_in_dim(residual, offset, half_width, 1)
    layer_out = (residual_half.astype(jnp.float32) + mix_gate[:, None] * dense + routed).astype(
        jnp.bfloat16
    )
    return (layer_out, new_keys, new_values)


def solution(mesh):
    finer = Mesh(mesh.devices.reshape(8, 4, 4, mesh.shape["tp"]), ("ep_0", "ep_1", "ep_2", "tp"))
    placed = (
        P(EP, None),
        P(EP),
        P(),
        P(None, "tp"),
        P(None, "tp"),
        P(None, "tp"),
        P("tp"),
        P(EP, "tp", None, None),
        P(EP, "tp", None, None),
        P("tp", None),
        P(),
        P(),
        P(EP, None),
        P(EP, "tp"),
        P(EP, "tp"),
        P("tp", EP),
        P(),
        P(EP, None, "tp"),
        P(EP, None, "tp"),
        P(EP, "tp", None),
    )
    return jax.shard_map(
        shards,
        mesh=finer,
        in_specs=placed,
        out_specs=(P(EP, "tp"), P(EP, "tp"), P(EP, "tp")),
        check_vma=False,
    )
```

profile of v0, /device:TPU:1, one launch (start us, length us, event | category | flops | bytes accessed | tf_op | source)
XLA Modules:
  0.0 185.2 jit_solution(10105115625662482061)
XLA Ops:
  7.2 0.0 all-gather.3.cloned.1.call-start
  7.2 1.5 pad_maximum_fusion
  8.7 1.3 reduce_max.9
  10.7 1.0 fusion.68
  11.7 2.1 %convolution_convert_fusion.4 = bf16[16,512]{1,0:T(8,128)(2,1)S(1)} fusion(bf16[2048,512]{1,0:T(8,128)(2,1)} %param.25, bf16[16,2048]{1,0:T(8,128)(2,1)} %param.22, f32[2048]{0:T(1024)} %param.24, f32[16]{0:T(128)S(1)} %add_rsqrt_fusion.1), kind=kOutput, calls=%fused_computation.53 | convolution fusion | flops 33693696 | bytes 2187328 | tf_op jit(solution)/shard_map/dot_general | solution.py:156
  13.8 0.1 reshape.249
  13.9 3.8 %while.15 = (s32[]{:T(128)}, f32[16,1,8,64]{3,2,0,1:T(8,128)S(1)}, f32[16,1,8]{0,2,1:T(8,128)S(1)}, s32[]{:T(128)}, s32[]{:T(128)}, /*index=5*/s32[16]{0:T(128)S...) while((s32[]{:T(128)}, f32[16,1,8,64]{3,2,0,1:T(8,128)S(1)}, ...), condition=%wide.region_4.5_spmd.clone, body=%wide.region_2.4_spmd.clone.sunk | while | flops 86458888 | bytes 3047731 | solution.py:114
  13.9 0.1 broadcast_compare_fusion.2
  14.0 1.6 fusion.112
  15.7 0.1 copy.97
  15.7 1.9 %fusion.113 = f32[16,1,8,64]{3,2,0,1:T(8,128)S(1)} fusion(f32[16,1,8,64]{3,2,0,1:T(8,128)S(1)} %get-tuple-element.330, bf16[16,1,64,1024]{3,2,0,1:T(8,128)(2,1)} %get-tuple-element.352, s32[]{:T(128)S(6)} %select_n.127, f32[16,8,512]{2,1,0:T(8,128)S(1)} %get-tuple-element.313, f32[16,8]{1,0:T(8,128)S(1)} %copy.97, ...), kind=kOutput, calls=%fused_computation.13.clone.1 | convolution fusion | flops 77340672 | bytes 1695748 | tf_op jit(solution)/shard_map/while/body/skgc,skdc->skgd/dot_general | solution.py:107
  17.6 0.1 copy.98
  17.7 0.0 copy-start.4
  17.8 0.1 convert_element_type.104
  17.9 0.4 convolution_convert_fusion.3
  18.2 0.7 broadcast_in_dim.40
  18.9 6.6 %all-to-all-start = ((bf16[2,16,2048]{2,1,0:T(8,128)(2,1)}), bf16[2,16,2048]{2,1,0:T(8,128)(2,1)S(1)}, u32[]{:S(2)}, u32[]{:S(2)}) async-start(bf16[2,16,2048]{2,1,0:T(8,128)(2,1)} %broadcast_in_dim.40), calls=%async_computation | async-start | bytes 262144 | tf_op jit(solution)/shard_map/all_to_all | solution.py:24
  25.5 0.1 copy.80
  25.6 0.1 eq.47
  25.7 0.2 convert_reduce_fusion.2
  25.9 0.5 copy-done.14
  26.4 0.1 reduce_sum.126
  26.4 0.1 copy.81
  26.5 0.1 fusion.74
  26.7 0.1 fusion.65
  26.8 1.5 convolution_convert_fusion.1
  28.3 1.7 reshape.252
  30.1 2.1 %constant_dynamic-slice_fusion = bf16[128,1,2048]{2,1,0:T(2,128)(2,1)} fusion(bf16[128,2,2048]{2,1,0:T(2,128)(2,1)S(1)} %reshape.252, s32[]{:T(128)S(6)} %select_n.73), kind=kLoop, calls=%fused_computation.119 | loop fusion | bytes 1048580 | tf_op jit(solution)/shard_map/dynamic_slice | solution.py:187
  32.1 0.5 broadcast.211
  32.6 4.8 %reduce.8 = bf16[128,2048]{1,0:T(8,128)(2,1)S(1)} reduce(bf16[128,1,2048]{2,1,0:T(2,128)(2,1)} %constant_dynamic-slice_fusion, bf16[]{:T(256)} %broadcast.211), dimensions={1}, to_apply=%constant_dynamic-slice_fusion.reduce_sub_computation | reduce | bytes 1048578 | tf_op jit(solution)/shard_map/dynamic_slice | solution.py:187
  37.4 1.2 reshape.275
  38.6 18.1 %all-to-all-start.2 = ((bf16[128,2,1024]{2,1,0:T(2,128)(2,1)}), bf16[128,2,1024]{2,1,0:T(2,128)(2,1)}, u32[]{:S(2)}, u32[]{:S(2)}) async-start(bf16[128,2,1024]{2,1,0:T(2,128)(2,1)} %reshape.275), calls=%async_computation.2 | async-start | bytes 1048576 | tf_op jit(solution)/shard_map/all_to_all | solution.py:54
  56.7 0.0 all-gather.5.cloned.1.call-start
  56.8 10.2 %all_gather.13 = bf16[256,64]{0,1:T(8,128)(2,1)S(1)} all-gather(bf16[256,16]{0,1:T(8,128)(2,1)S(1)} %copy-done.8), channel_id=1, replica_groups=mesh['ep_0'=8,'ep_1'=4,'ep_2'=4,'tp'=2] {'ep_2'}, dimensions={1}, use_global_device_ids=true | all-gather | bytes 40960 | tf_op jit(solution)/shard_map/all_gather | solution.py:71
  67.0 10.7 %all_gather.14 = bf16[256,256]{0,1:T(8,128)(2,1)} all-gather(bf16[256,64]{0,1:T(8,128)(2,1)S(1)} %all_gather.13), channel_id=1, replica_groups=mesh['ep_0'=8,'ep_1'=4,'ep_2'=4,'tp'=2] {'ep_1'}, dimensions={1}, use_global_device_ids=true | all-gather | bytes 163840 | tf_op jit(solution)/shard_map/all_gather | solution.py:71
  77.7 0.6 reshape.261
  78.3 0.3 fusion.50
  78.5 0.2 select_reduce_fusion
  78.7 0.1 copy.79
  78.8 3.6 %reshape.276 = bf16[128,1,2048]{2,1,0:T(2,128)(2,1)S(1)} reshape(bf16[128,2,1024]{2,1,0:T(2,128)(2,1)} %all-to-all-done.2) | data formatting | bytes 1048576
  82.4 0.3 copy.93
  82.7 0.1 broadcast_in_dim.43
  82.9 9.0 %all_to_all.33 = bf16[2,128,1,2048]{3,1,2,0:T(8,128)(2,1)S(1)} all-to-all(bf16[2,128,1,2048]{3,1,2,0:T(8,128)(2,1)S(1)} %broadcast_in_dim.43), channel_id=1, replica_groups=mesh['ep_0'=8,'ep_1'=4,'ep_2'=4,'tp'=2] {'tp'}, dimensions={0} | all-to-all | bytes 2097152 | tf_op jit(solution)/shard_map/all_to_all | solution.py:24
  91.9 0.4 convolution_bitcast_fusion.1
  92.3 3.8 %convolution_convert_fusion = bf16[256,2048]{1,0:T(8,128)(2,1)} fusion(bf16[1,256,2048]{2,1,0:T(8,128)(2,1)} %param.41, bf16[256,2048]{1,0:T(8,128)(2,1)S(1)} %bitcast.128, bf16[1,2048,256]{2,1,0:T(8,128)(2,1)} %param.40, f32[256,1,1,256]{3,0,2,1:T(8,128)S(1)} %convolution_bitcast_fusion.1), kind=kOutput, calls=%fused_computation.44 | convolution fusion | flops 537788416 | bytes 4456448 | tf_op jit(solution)/shard_map/njcf,jfd->njcd/dot_general | solution.py:124
  96.1 1.3 copy.92
  97.4 4.5 %all_to_all.34 = bf16[2,256,1,1,1024]{4,1,3,2,0:T(8,128)(2,1)S(1)} all-to-all(bf16[2,256,1,1,1024]{4,1,3,2,0:T(8,128)(2,1)S(1)} %bitcast.129), channel_id=1, replica_groups=mesh['ep_0'=8,'ep_1'=4,'ep_2'=4,'tp'=2] {'tp'}, dimensions={0} | all-to-all | bytes 2097152 | tf_op jit(solution)/shard_map/all_to_all | solution.py:18
  102.0 1.2 reduce_sum.128
  103.1 2.4 %copy.83 = bf16[2,128,1,1024]{3,0,2,1:T(2,128)(2,1)} copy(bf16[2,128,1,1024]{3,1,0,2:T(8,128)(2,1)} %bitcast.131) | data formatting | bytes 1048576 | tf_op jit(solution)/shard_map/reshape | solution.py:195
  105.6 12.7 %all-to-all-start.5 = ((bf16[2,128,1,1024]{3,0,2,1:T(2,128)(2,1)}), bf16[2,128,1,1024]{3,0,2,1:T(2,128)(2,1)S(1)}, u32[]{:S(2)}, u32[]{:S(2)}) async-start(bf16[2,128,1,1024]{3,0,2,1:T(2,128)(2,1)} %copy.83), calls=%async_computation.5 | async-start | bytes 1048576 | tf_op jit(solution)/shard_map/all_to_all | solution.py:198
  118.3 0.2 multiply_reduce_fusion.1
  118.6 0.8 convolution_convert_fusion.6
  119.4 0.8 convolution_convert_fusion.5
  120.2 19.1 %all-to-all-done.5 = bf16[2,128,1,1024]{3,0,2,1:T(2,128)(2,1)S(1)} async-done(((bf16[2,128,1,1024]{3,0,2,1:T(2,128)(2,1)}), bf16[2,128,1,1024]{3,0,2,1:T(2,128)(2,1)S(1)}, u32[]{:S(2)}, u32[]{:S(2)}) %all-to-all-start.5) | async-done | bytes 524320 | tf_op jit(solution)/shard_map/all_to_all | solution.py:198
  139.3 0.1 copy.84
  139.5 0.8 gather_fusion
  140.3 0.1 reshape.262
  140.3 0.2 multiply_reduce_fusion
  140.5 0.0 all-gather.3.cloned.1.call-done
  140.6 1.5 fusion.53
  142.1 24.0 %all-gather.5.cloned.1.call-done = bf16[256,2048]{0,1:T(8,128)(2,1)} async-done(((bf16[256,256]{0,1:T(8,128)(2,1)}), bf16[256,2048]{0,1:T(8,128)(2,1)}) %all-gather.5.cloned.1.call-update) | async-done | bytes 1048592 | tf_op jit(solution)/shard_map/all_gather | solution.py:71
  166.1 2.4 %convolution_convert_fusion.2 = bf16[16,2048]{1,0:T(8,128)(2,1)S(1)} fusion(bf16[256,2048]{0,1:T(8,128)(2,1)} %all-gather.5.cloned.1.call-done, bf16[2048,512]{1,0:T(8,128)(2,1)} %all-gather.3.cloned.1.call-done, f32[16,256]{1,0:T(8,128)S(1)} %fusion.53, bf16[16,2048]{1,0:T(8,128)(2,1)S(1)} %get-tuple-element.246, f32[2048]{0:T(1024)S(1)} %copy-done.4, ...), kind=kOutput, calls=%fused_computation.46 | convolution fusion | flops 33742848 | bytes 2252864 | tf_op jit(solution)/shard_map/dot_general | solution.py:214
  168.5 9.2 %all_to_all.35 = bf16[2,16,1024]{2,1,0:T(8,128)(2,1)S(1)} all-to-all(bf16[2,16,1024]{2,1,0:T(8,128)(2,1)S(1)} %bitcast.135), channel_id=1, replica_groups=mesh['ep_0'=8,'ep_1'=4,'ep_2'=4,'tp'=2] {'tp'}, dimensions={0} | all-to-all | bytes 131072 | tf_op jit(solution)/shard_map/all_to_all | solution.py:18
  177.7 0.7 add_convert_fusion
  (57 shorter events, 0.3 us)
Async XLA Ops:
  7.2 10.7 %copy-start = (bf16[512,2048]{1,0:T(8,128)(2,1)S(1)}, bf16[512,2048]{1,0:T(8,128)(2,1)}, u32[]{:S(2)}) copy-start(bf16[512,2048]{1,0:T(8,128)(2,1)} %param.31) | copy-start | bytes 6291460
  7.2 6.7 %copy-start.6 = (s32[16]{0:T(128)S(1)}, s32[16]{0:T(128)}, u32[]{:S(2)}) copy-start(s32[16]{0:T(128)} %param.23) | copy-start | bytes 196
  7.2 6.7 %copy-start.19 = (f32[8]{0:T(128)S(1)}, f32[8]{0:T(128)}, u32[]{:S(2)}) copy-start(f32[8]{0:T(128)} %param.28) | copy-start | bytes 100
  7.2 133.4 %all-gather.3.cloned.1.call-start = ((), (), s32[]{:S(2)}) async-start(), calls=%async_computation.6 | async-start | bytes 2113536 | tf_op jit(solution)/shard_map/all_gather | solution.py:65
  11.7 2.2 %copy-start.12 = (f32[16]{0:T(128)}, f32[16]{0:T(128)S(1)}, u32[]{:S(2)}) copy-start(f32[16]{0:T(128)S(1)} %add_rsqrt_fusion.1) | copy-start | bytes 196
  17.7 7.8 %copy-start.5 = (s32[16,6]{0,1:T(8,128)S(1)}, s32[16,6]{0,1:T(8,128)}, u32[]{:S(2)}) copy-start(s32[16,6]{0,1:T(8,128)} %param.34) | copy-start | bytes 1156
  17.7 9.0 %copy-start.2 = (bf16[16,2048]{1,0:T(8,128)(2,1)S(1)}, bf16[16,2048]{1,0:T(8,128)(2,1)}, u32[]{:S(2)}) copy-start(bf16[16,2048]{1,0:T(8,128)(2,1)} %param.22) | copy-start | bytes 196612
  17.7 9.1 %copy-start.4 = (f32[2048]{0:T(1024)S(1)}, f32[2048]{0:T(1024)}, u32[]{:S(2)}) copy-start(f32[2048]{0:T(1024)} %param.32) | copy-start | bytes 24580
  18.9 7.7 %all-to-all-start = ((bf16[2,16,2048]{2,1,0:T(8,128)(2,1)}), bf16[2,16,2048]{2,1,0:T(8,128)(2,1)S(1)}, u32[]{:S(2)}, u32[]{:S(2)}) async-start(bf16[2,16,2048]{2,1,0:T(8,128)(2,1)} %broadcast_in_dim.40), calls=%async_computation | async-start | bytes 262144 | tf_op jit(solution)/shard_map/all_to_all | solution.py:24
  25.8 0.5 copy-start.14
  26.8 51.4 %copy-start.10 = (f32[16]{0:T(128)}, f32[16]{0:T(128)S(1)}, u32[]{:S(2)}) copy-start(f32[16]{0:T(128)S(1)} %add_rsqrt_fusion) | copy-start | bytes 196
  32.1 24.7 %copy-start.8 = (bf16[256,16]{0,1:T(8,128)(2,1)S(1)}, bf16[256,16]{0,1:T(8,128)(2,1)}, u32[]{:S(2)}) copy-start(bf16[256,16]{0,1:T(8,128)(2,1)} %param.37) | copy-start | bytes 24580
  32.1 46.1 %copy-start.3 = (bf16[2048,128]{1,0:T(8,128)(2,1)S(1)}, bf16[2048,128]{1,0:T(8,128)(2,1)}, u32[]{:S(2)}) copy-start(bf16[2048,128]{1,0:T(8,128)(2,1)} %param.33) | copy-start | bytes 1572868
  38.6 40.2 %all-to-all-start.2 = ((bf16[128,2,1024]{2,1,0:T(2,128)(2,1)}), bf16[128,2,1024]{2,1,0:T(2,128)(2,1)}, u32[]{:S(2)}, u32[]{:S(2)}) async-start(bf16[128,2,1024]{2,1,0:T(2,128)(2,1)} %reshape.275), calls=%async_computation.2 | async-start | bytes 1048576 | tf_op jit(solution)/shard_map/all_to_all | solution.py:54
  56.7 109.3 %all-gather.5.cloned.1.call-start = ((), (), s32[]{:S(2)}) async-start(), calls=%async_computation.7 | async-start | bytes 1179648 | tf_op jit(solution)/shard_map/all_gather | solution.py:71
  82.7 9.2 %copy-start.1 = (bf16[1,2048,256]{2,1,0:T(8,128)(2,1)S(1)}, bf16[1,2048,256]{2,1,0:T(8,128)(2,1)}, u32[]{:S(2)}) copy-start(bf16[1,2048,256]{2,1,0:T(8,128)(2,1)} %param.39) | copy-start | bytes 3145732
  102.0 16.3 %copy-start.15 = (s32[96]{0:T(128)S(1)}, s32[96]{0:T(128)}, u32[]{:S(2)}) copy-start(s32[96]{0:T(128)} %copy-done.14) | copy-start | bytes 1156
  102.0 16.3 %copy-start.16 = (s32[96,1]{0,1:T(1,128)S(1)}, s32[96,1]{0,1:T(1,128)}, u32[]{:S(2)}) copy-start(s32[96,1]{0,1:T(1,128)} %reshape.261) | copy-start | bytes 1156
  102.0 16.3 %copy-start.9 = (f32[2048]{0:T(1024)S(1)}, f32[2048]{0:T(1024)}, u32[]{:S(2)}) copy-start(f32[2048]{0:T(1024)} %param.38) | copy-start | bytes 24580
  102.0 16.3 %copy-start.11 = (f32[16]{0:T(128)S(1)}, f32[16]{0:T(128)}, u32[]{:S(2)}) copy-start(f32[16]{0:T(128)} %copy-done.10) | copy-start | bytes 196
  102.0 16.6 %copy-start.7 = (f32[2048]{0:T(1024)S(1)}, f32[2048]{0:T(1024)}, u32[]{:S(2)}) copy-start(f32[2048]{0:T(1024)} %param.24) | copy-start | bytes 24580
  102.0 16.6 %copy-start.13 = (f32[16]{0:T(128)S(1)}, f32[16]{0:T(128)}, u32[]{:S(2)}) copy-start(f32[16]{0:T(128)} %copy-done.12) | copy-start | bytes 196
  103.1 15.4 %copy-start.17 = (bf16[2048,64]{0,1:T(8,128)(2,1)S(1)}, bf16[2048,64]{0,1:T(8,128)(2,1)}, u32[]{:S(2)}) copy-start(bf16[2048,64]{0,1:T(8,128)(2,1)} %param.26) | copy-start | bytes 786436
  103.1 16.2 %copy-start.18 = (bf16[2048,64]{0,1:T(8,128)(2,1)S(1)}, bf16[2048,64]{0,1:T(8,128)(2,1)}, u32[]{:S(2)}) copy-start(bf16[2048,64]{0,1:T(8,128)(2,1)} %param.27) | copy-start | bytes 786436
  105.6 33.8 %all-to-all-start.5 = ((bf16[2,128,1,1024]{3,0,2,1:T(2,128)(2,1)}), bf16[2,128,1,1024]{3,0,2,1:T(2,128)(2,1)S(1)}, u32[]{:S(2)}, u32[]{:S(2)}) async-start(bf16[2,128,1,1024]{3,0,2,1:T(2,128)(2,1)} %copy.83), calls=%async_computation.5 | async-start | bytes 1048576 | tf_op jit(solution)/shard_map/all_to_all | solution.py:198
Sparse Core Ops, SparseCore 0:
  12.2 116.3 all-gather.2
  130.3 35.6 all-gather.4
where the time goes:
time: 186 us; the launch traced here: 185 us
  blocking collectives  43.5 us (23%)
  waiting for transfers between devices  43.2 us (23%)
  starting transfers between devices  37.4 us (20%)
  matrix products  17.5 us (9%)
  local copies, waits for them, and re-layouts  16.9 us (9%)
  between operations  15.1 us (8%)
  other arithmetic  11.6 us (6%)
    all_gather x1, waiting for transfers between devices, gather_axes(): x = lax.all_gather(x, axis, axis=dim, tiled=True)  24 us
    all_gather x2, blocking collectives, gather_axes(): x = lax.all_gather(x, axis, axis=dim, tiled=True)  20.8 us
    all_to_all x1, waiting for transfers between devices, run_halves(): return lax.all_to_all(summed, EP, split_axis=1, concat_axis=1, tiled=True)  19.1 us
    all_to_all x1, starting transfers between devices, grouped_exchange(): lax.all_to_all(group, axis, split_axis=split_dim, concat_axis=concat_dim,...  18.1 us
    all_to_all x2, blocking collectives, sum_at_owner(): parts = lax.all_to_all(cut_along(x, dim, size), axis, 0, 0, tiled=True)  13.7 us
    all_to_all x1, starting transfers between devices, run_halves(): return lax.all_to_all(summed, EP, split_axis=1, concat_axis=1, tiled=True)  12.7 us
    all_to_all x1, blocking collectives, from_everyone(): return lax.all_to_all(copies, axis, split_axis=0, concat_axis=0, tiled=True)  9.02 us
    all_to_all x1, starting transfers between devices, from_everyone(): return lax.all_to_all(copies, axis, split_axis=0, concat_axis=0, tiled=True)  6.57 us
  transfers between devices with their start and end apart: 5, of which 2 were waited for; matrix products, arithmetic and copies ran while one was open for 22% of the time, Pallas kernels for 0%

commit v1 on v0

v1 whole, which is shorter than its diff:
```python
import jax
import jax.numpy as jnp
from jax import lax
from jax.experimental import pallas as pl
from jax.experimental.pallas import tpu as pltpu
from jax.sharding import Mesh
from jax.sharding import PartitionSpec as P

EP = ("z", "y", "x")
MESH = pl.DeviceIdType.MESH
NZ, NY, NX = 8, 4, 4
PLANE = NY * NX
ROWS, WIDTH, HALF = 16, 2048, 1024
F32, BF16 = jnp.float32, jnp.bfloat16
NT = (((1,), (1,)), ((), ()))
LOADS = 21


def dot(a, b):
    return jnp.dot(a, b, preferred_element_type=F32)


def dot_nt(a, b):
    return lax.dot_general(a, b, NT, preferred_element_type=F32)


def iota(shape, dim):
    return lax.broadcasted_iota(jnp.int32, shape, dim)


def bits(mask):
    return jnp.where(mask, 1.0, 0.0).astype(BF16)


def two_terms(x):
    high = x.astype(BF16)
    return high, (x - high.astype(F32)).astype(BF16)


def sigmoid(x):
    return 1.0 / (1.0 + jnp.exp(-x))


def rms_scale(values, gain):
    wide = values.astype(F32)
    return (wide * lax.rsqrt(jnp.mean(wide * wide, axis=-1, keepdims=True) + 1e-06) * gain).astype(BF16)


def kernel(
    tokens_h, lengths, attn_gain_h, wq_h, wk_h, wv_h, head_bias, keys_h, values_h, wo_h,
    ffn_gain_h, wr_h, routes_h, wdg_h, wdu_h, wdd_h, mix_h, weg_h, weu_h, wed_h,
    out, new_keys, new_values,
    tokens, attn_gain, wq, wk, wv, keys, values, wo, ffn_gain, wr, routes, wdg, wdu, wdd, mixw,
    weg, weu, wed,
    w3p, w3, hits, gm, part, peer_part, norm2, resid, tokf, xs, xin, eo_mine, eo_send, eo_peer,
    ys, yr, dn_mine, dn_send, dn_peer, ps, pr,
    load_sem, w3z_s, w3z_r, w3x_s, w3x_r, w3y_s, w3y_r, h_s, h_r, ap_s, ap_r, tz_s, tz_r, g_s, g_r,
    tf_s, tf_r, xs_s, xs_r, xf_s, xf_r, eo_s, eo_r, ys_s, ys_r, dn_s, dn_r, ps_s, ps_r,
):
    z, y, x, t = (lax.axis_index(a) for a in ("z", "y", "x", "tp"))

    def at_z(dz):
        return (lax.rem(z + dz, NZ), y, x, t)

    def at_y(dy):
        return (z, lax.rem(y + dy, NY), x, t)

    def at_x(dx):
        return (z, y, lax.rem(x + dx, NX), t)

    def in_plane(d):
        return (z, lax.rem(y + d // NX, NY), lax.rem(x + d % NX, NX), t)

    def back_in_plane(d):
        return (z, lax.rem(y + NY - d // NX, NY), lax.rem(x + NX - d % NX, NX), t)

    partner = (z, y, x, 1 - t)

    def remote(src, dst, s, r, device):
        return pltpu.make_async_remote_copy(
            src_ref=src, dst_ref=dst, send_sem=s, recv_sem=r, device_id=device, device_id_type=MESH
        )

    barrier = pltpu.get_barrier_semaphore()
    others = [at_z(d) for d in range(1, NZ)] + [in_plane(d) for d in range(1, PLANE)] + [partner]
    for device in others:
        pl.semaphore_signal(barrier, inc=1, device_id=device, device_id_type=MESH)

    loads = []

    def load(src, dst):
        copy = pltpu.make_async_copy(src, dst, load_sem.at[len(loads)])
        copy.start()
        loads.append(copy)
        return copy

    ld_dense = [load(wdg_h, wdg), load(wdu_h, wdu), load(wdd_h, wdd), load(routes_h, routes)]
    ld_tok = [load(tokens_h, tokens), load(attn_gain_h, attn_gain)]
    ld_q = load(wq_h, wq)
    ld_kv = [load(wk_h, wk), load(wv_h, wv)]
    ld_keys = load(keys_h, keys)
    ld_values = load(values_h, values)
    ld_wo = load(wo_h, wo)
    ld_n2 = [load(ffn_gain_h, ffn_gain), load(mix_h, mixw), load(wr_h, wr)]
    ld_eg = [load(weg_h, weg), load(weu_h, weu)]
    ld_ed = [load(wed_h.at[:, pl.ds(h * HALF, HALF)], wed.at[h]) for h in range(2)]

    for copy in ld_dense:
        copy.wait()
    lane = iota((1, NZ * 128), 1)
    first = lax.rem(z + lane // 128, NZ) * 32
    within = lane % 128
    unit = iota((256, NZ * 128), 0)
    eye = bits(iota((ROWS, ROWS), 0) == iota((ROWS, ROWS), 1))
    down_t = dot_nt(eye, wdd[...]).astype(BF16)
    pieces = jnp.zeros((ROWS, NZ * 128), F32)
    for k, w in enumerate((wdg[...], wdu[...], down_t)):
        target = jnp.where((within >= 32 * k) & (within < 32 * k + 32), first + within - 32 * k, -1)
        pieces = pieces + dot(w, bits(unit == target))
    pieces = pieces.astype(BF16)
    for dz in range(NZ):
        w3p[dz] = pieces[:, dz * 128 : (dz + 1) * 128]
    own_hits = jnp.zeros((ROWS, 128), F32)
    for k in range(routes.shape[1]):
        own_hits = own_hits + jnp.where(routes[:, k : k + 1] == iota((ROWS, 128), 1), 1.0, 0.0)
    hits[0] = own_hits.astype(BF16)
    w3[z, y, x] = w3p[0]

    for copy in ld_tok:
        copy.wait()
    normed = rms_scale(tokens[...], attn_gain[...])
    ld_q.wait()
    queries = dot(normed, wq[...]).astype(BF16)
    for copy in ld_kv:
        copy.wait()
    new_keys[...] = dot(normed, wk[...]).astype(BF16)
    new_values[...] = dot(normed, wv[...]).astype(BF16)

    pl.semaphore_wait(barrier, len(others))
    w3z = [remote(w3p.at[d], w3.at[z, y, x], w3z_s.at[d], w3z_r.at[d], at_z(d)) for d in range(1, NZ)]
    hz = [remote(hits.at[0], hits.at[d], h_s.at[d], h_r.at[d], at_z(d)) for d in range(1, NZ)]
    for copy in w3z + hz:
        copy.start()
    w3x = [remote(w3.at[:, y, x], w3.at[:, y, x], w3x_s.at[d], w3x_r.at[d], at_x(d)) for d in range(1, NX)]
    w3y = [remote(w3.at[:, y], w3.at[:, y], w3y_s.at[d], w3y_r.at[d], at_y(d)) for d in range(1, NY)]

    row = iota((128, 1), 0)
    rep = bits(iota((128, ROWS), 0) // 8 == iota((128, ROWS), 1))
    head_lane = iota((128, 512), 1) // 64 == iota((128, 512), 0) % 8
    fold = bits(iota((512, 256), 0) % 64 == iota((512, 256), 1) % 64)
    own_block = iota((128, 256), 1) // 64 == (iota((128, 256), 0) // 8) % 4
    spread = jnp.where(head_lane, dot(rep, queries), 0.0).astype(BF16)
    block_q = jnp.where(own_block, dot(spread, fold), 0.0).astype(BF16)
    bias = jnp.zeros((32, 1), F32)
    for h in range(8):
        bias = jnp.where(iota((32, 1), 0) % 8 == h, head_bias[h], bias)
    after = bits(iota((256, 256), 0) > iota((256, 256), 1))
    ld_keys.wait()
    ld_values.wait()
    mixed = []
    for g in range(4):
        scores = dot(block_q[g * 32 : (g + 1) * 32], keys[pl.ds(g * 256, 256), :]) * 0.125 + bias
        length = jnp.zeros((32, 1), jnp.int32)
        for s in range(4):
            length = jnp.where(iota((32, 1), 0) // 8 == s, lengths[g * 4 + s], length)
        visible = iota((32, 1024), 1) < length
        soft = jnp.log1p(jnp.exp(-jnp.abs(scores)))
        log_take = jnp.minimum(scores, 0.0) - soft
        log_keep = jnp.where(visible, jnp.minimum(-scores, 0.0) - soft, 0.0)
        tiles = jnp.concatenate([log_keep[:, j * 256 : (j + 1) * 256] for j in range(4)], axis=0)
        high, low = two_terms(tiles)
        summed = dot(high, after) + dot(low, after)
        total = summed[:, 0:1] + tiles[:, 0:1]
        later = jnp.zeros((32, 1), F32)
        spans = [None] * 4
        for j in reversed(range(4)):
            spans[j] = summed[j * 32 : (j + 1) * 32] + later
            later = later + total[j * 32 : (j + 1) * 32]
        log_after = jnp.concatenate(spans, axis=1)
        stick = jnp.where(visible, jnp.exp(log_take + log_after), 0.0).astype(BF16)
        mixed.append(dot_nt(stick, values[pl.ds(g * 256, 256), :]))
        if g == 1:
            for copy in w3z:
                copy.wait_recv()
            for copy in w3x:
                copy.start()
        if g == 2:
            for copy in w3x:
                copy.wait_recv()
            for copy in w3y:
                copy.start()
    mixed = jnp.where(own_block, jnp.concatenate(mixed, axis=0), 0.0).astype(BF16)
    unfold = bits(iota((256, 512), 0) % 64 == iota((256, 512), 1) % 64)
    by_head = jnp.where(head_lane, dot(mixed, unfold), 0.0).astype(BF16)
    gather_rows = bits(iota((ROWS, 128), 1) // 8 == iota((ROWS, 128), 0))
    heads_out = dot(gather_rows, by_head).astype(BF16)
    ld_wo.wait()
    part[...] = dot(heads_out, wo[...]).astype(BF16)
    ap = remote(part, peer_part, ap_s.at[0], ap_r.at[0], partner)
    ap.start()

    for copy in hz:
        copy.wait_recv()
    hit = hits[...].reshape(128, 128)
    base = z * PLANE

    def expert_of(slot):
        d = slot // 16
        return base + lax.rem(y + d // NX, NY) * NX + lax.rem(x + d % NX, NX)

    sel = bits(iota((256, 128), 1) == expert_of(iota((256, 128), 0)))
    tok_r, tok_c = iota((128, 128), 0), iota((128, 128), 1)
    earlier_c = bits((tok_r < tok_c) & (tok_r // 16 == tok_c // 16))
    earlier_r = bits((tok_c < tok_r) & (tok_r // 16 == tok_c // 16))
    slot_hit = dot_nt(sel, hit)
    slot_rank = dot(slot_hit.astype(BF16), earlier_c)
    sr, sc = iota((256, 128), 0), iota((256, 128), 1)
    fits = (slot_rank == ((sr // 8) % 2).astype(F32)) & (sc // 16 == sr % 8)
    dispatch = jnp.where(fits, slot_hit, 0.0).astype(BF16)
    tok_hit = dot_nt(hit, sel)
    tok_rank = dot_nt(dot(earlier_r, hit).astype(BF16), sel)
    cr, cc = iota((128, 256), 0), iota((128, 256), 1)
    taken = (tok_rank == ((cc // 8) % 2).astype(F32)) & (cr // 16 == cc % 8) & (tok_hit > 0.5)

    for copy in ld_n2:
        copy.wait()
    ap.wait_recv()
    residual = (tokens[...].astype(F32) + (part[...].astype(F32) + peer_part[...].astype(F32))).astype(BF16)
    normed2 = rms_scale(residual, ffn_gain[...])
    for h in range(2):
        norm2[h] = normed2[:, h * HALF : (h + 1) * HALF]
        resid[h] = residual[:, h * HALF : (h + 1) * HALF]
    tokf[t, 0] = norm2[t]
    tz = [remote(norm2.at[t], tokf.at[t, d], tz_s.at[d], tz_r.at[d], at_z(d)) for d in range(1, NZ)]
    for d in (4, 3, 5, 2, 6, 1, 7):
        tz[d - 1].start()
    probs = sigmoid(dot(normed2, wr[...]))
    picked = own_hits * probs
    gates = picked / jnp.sum(picked, axis=-1, keepdims=True) * 2.5
    mix = sigmoid(jnp.sum(normed2.astype(F32) * mixw[...], axis=-1, keepdims=True))
    gm[0] = jnp.concatenate([gates, jnp.broadcast_to(mix, (ROWS, 128))], axis=1)
    gz = [remote(gm.at[0], gm.at[d], g_s.at[d], g_r.at[d], at_z(d)) for d in range(1, NZ)]
    for copy in gz:
        copy.start()

    for copy in tz:
        copy.wait_recv()
    rows = dot(dispatch, tokf[t].reshape(128, HALF)).astype(BF16).reshape(PLANE, 16, HALF)
    for d in range(1, PLANE):
        xs[d] = rows[d]
    xin[t, 0] = rows[0]
    xd = [remote(xs.at[d], xin.at[t, d], xs_s.at[d], xs_r.at[d], in_plane(d)) for d in range(1, PLANE)]
    order = sorted(range(1, PLANE), key=lambda d: -(min(d // NX, NY - d // NX) + min(d % NX, NX - d % NX)))
    for d in order:
        xd[d - 1].start()
    tf = remote(tokf.at[t], tokf.at[t], tf_s.at[0], tf_r.at[0], partner)
    tf.start()
    xf = [remote(xin.at[t, d], xin.at[t, d], xf_s.at[d], xf_r.at[d], partner) for d in range(PLANE)]
    xf[0].start()

    for copy in w3y:
        copy.wait_recv()
    tf.wait_recv()
    lo, hi = w3[0:4].reshape(HALF, 128), w3[4:8].reshape(HALF, 128)
    pre = dot(tokf[0].reshape(128, HALF), lo) + dot(tokf[1].reshape(128, HALF), hi)
    gate_in, up_in = pltpu.roll(pre, 64, 1), pltpu.roll(pre, 32, 1)
    used = (iota((128, 128), 1) >= 64) & (iota((128, 128), 1) < 96)
    dense_hidden = jnp.where(used, gate_in * sigmoid(gate_in) * up_in, 0.0).astype(BF16)
    dn_send[...] = dot_nt(dense_hidden, w3[pl.ds(4 * (1 - t), 4)].reshape(HALF, 128)).astype(BF16)
    dn = remote(dn_send, dn_peer, dn_s.at[0], dn_r.at[0], partner)
    dn.start()
    dn_mine[...] = dot_nt(dense_hidden, w3[pl.ds(4 * t, 4)].reshape(HALF, 128)).astype(BF16)

    for d in reversed(order):
        xd[d - 1].wait_recv()
        xf[d].start()
    for copy in ld_eg:
        copy.wait()
    mine = xin[t].reshape(256, HALF)
    gate_mine = dot(mine, weg[t])
    up_mine = dot(mine, weu[t])
    for copy in xf:
        copy.wait_recv()
    theirs = xin[1 - t].reshape(256, HALF)
    gate_rows = gate_mine + dot(theirs, weg[1 - t])
    up_rows = up_mine + dot(theirs, weu[1 - t])
    hidden = (gate_rows * sigmoid(gate_rows) * up_rows).astype(BF16)
    for copy in ld_ed:
        copy.wait()
    eo_send[...] = dot(hidden, wed[1 - t]).astype(BF16)
    eo = remote(eo_send, eo_peer, eo_s.at[0], eo_r.at[0], partner)
    eo.start()
    eo_mine[...] = dot(hidden, wed[t]).astype(BF16)

    for copy in gz:
        copy.wait_recv()
    gmv = gm[...].reshape(128, 256)
    gate_high, gate_low = two_terms(gmv[:, 0:128])
    slot_gate = jnp.where(taken, dot_nt(gate_high, sel) + dot_nt(gate_low, sel), 0.0)
    comb_high, comb_low = two_terms(slot_gate)
    dn.wait_recv()
    dense = gmv[:, 128:129] * (dn_mine[...].astype(F32) + dn_peer[...].astype(F32))

    eo.wait_recv()
    done = (eo_mine[...].astype(F32) + eo_peer[...].astype(F32)).astype(BF16).reshape(PLANE, 16, HALF)
    for d in range(1, PLANE):
        ys[d] = done[d]
    yr[0] = done[0]
    yd = [remote(ys.at[d], yr.at[d], ys_s.at[d], ys_r.at[d], back_in_plane(d)) for d in range(1, PLANE)]
    for d in order:
        yd[d - 1].start()
    for copy in yd:
        copy.wait_recv()
    back = yr[...].reshape(256, HALF)
    sums = dense + (dot(comb_high, back) + dot(comb_low, back))
    sums3 = sums.astype(BF16).reshape(NZ, ROWS, HALF)
    for d in range(1, NZ):
        ps[d] = sums3[d]
    zd = [
        remote(ps.at[d], pr.at[d], ps_s.at[d], ps_r.at[d], at_z(NZ - d)) for d in range(1, NZ)
    ]
    for d in (4, 3, 5, 2, 6, 1, 7):
        zd[d - 1].start()
    total_out = resid[t].astype(F32) + sums[0:ROWS]
    for copy in zd:
        copy.wait_recv()
    for d in range(1, NZ):
        total_out = total_out + pr[d].astype(F32)
    out[...] = total_out.astype(BF16)
    for copy in [*w3z, *hz, *w3x, *w3y, ap, *tz, *gz, tf, *xd, *xf, dn, eo, *yd, *zd]:
        copy.wait_send()


def shards(
    tokens, lengths, attn_gain, w_query, w_key, w_value, head_bias, key_cache, value_cache, w_attn_out,
    ffn_gain, w_router, routes, w_dense_gate, w_dense_up, w_dense_down, dense_mix,
    w_expert_gate, w_expert_up, w_expert_down,
):
    args = (
        tokens, lengths, attn_gain.reshape(1, WIDTH), w_query, w_key, w_value, head_bias,
        key_cache.reshape(1024, 1024), value_cache.reshape(1024, 1024), w_attn_out,
        ffn_gain.reshape(1, WIDTH), w_router, routes, w_dense_gate, w_dense_up, w_dense_down,
        dense_mix.reshape(1, WIDTH), w_expert_gate.reshape(2, HALF, 256), w_expert_up.reshape(2, HALF, 256),
        w_expert_down.reshape(256, WIDTH),
    )
    smem = {1, 6}
    vm, dma = pltpu.VMEM, pltpu.SemaphoreType.DMA
    scratch = [
        vm((ROWS, WIDTH), BF16), vm((1, WIDTH), F32), vm((WIDTH, 512), BF16), vm((WIDTH, 64), BF16),
        vm((WIDTH, 64), BF16), vm((1024, 1024), BF16), vm((1024, 1024), BF16), vm((512, WIDTH), BF16),
        vm((1, WIDTH), F32), vm((WIDTH, 128), BF16), vm((ROWS, 6), jnp.int32), vm((ROWS, 256), BF16),
        vm((ROWS, 256), BF16), vm((256, ROWS), BF16), vm((1, WIDTH), F32),
        vm((2, HALF, 256), BF16), vm((2, HALF, 256), BF16), vm((2, 256, HALF), BF16),
        vm((NZ, ROWS, 128), BF16), vm((NZ, NY, NX, ROWS, 128), BF16), vm((NZ, ROWS, 128), BF16),
        vm((NZ, ROWS, 256), F32), vm((ROWS, WIDTH), BF16), vm((ROWS, WIDTH), BF16),
        vm((2, ROWS, HALF), BF16), vm((2, ROWS, HALF), BF16), vm((2, NZ, ROWS, HALF), BF16),
        vm((PLANE, 16, HALF), BF16), vm((2, PLANE, 16, HALF), BF16),
        vm((256, HALF), BF16), vm((256, HALF), BF16), vm((256, HALF), BF16),
        vm((PLANE, 16, HALF), BF16), vm((PLANE, 16, HALF), BF16),
        vm((128, HALF), BF16), vm((128, HALF), BF16), vm((128, HALF), BF16),
        vm((NZ, ROWS, HALF), BF16), vm((NZ, ROWS, HALF), BF16),
        dma((LOADS,)),
    ]
    for n in (NZ, NX, NY, NZ, 1, NZ, NZ, 1, PLANE, PLANE, 1, PLANE, 1, NZ):
        scratch += [dma((n,)), dma((n,))]
    return pl.pallas_call(
        kernel,
        out_shape=(
            jax.ShapeDtypeStruct((ROWS, HALF), BF16),
            jax.ShapeDtypeStruct((ROWS, 64), BF16),
            jax.ShapeDtypeStruct((ROWS, 64), BF16),
        ),
        in_specs=[
            pl.BlockSpec(memory_space=pltpu.SMEM if k in smem else pl.ANY) for k in range(len(args))
        ],
        out_specs=tuple(pl.BlockSpec(memory_space=pltpu.VMEM) for _ in range(3)),
        scratch_shapes=scratch,
        compiler_params=pltpu.CompilerParams(
            collective_id=0, has_side_effects=True, vmem_limit_bytes=60 * 1024 * 1024
        ),
    )(*args)


def solution(mesh):
    finer = Mesh(mesh.devices.reshape(NZ, NY, NX, mesh.shape["tp"]), ("z", "y", "x", "tp"))
    placed = (
        P(EP, None), P(EP), P(), P(None, "tp"), P(None, "tp"), P(None, "tp"), P("tp"),
        P(EP, "tp", None, None), P(EP, "tp", None, None), P("tp", None), P(), P(), P(EP, None),
        P(EP, "tp"), P(EP, "tp"), P("tp", EP), P(), P(EP, None, "tp"), P(EP, None, "tp"), P(EP, "tp", None),
    )
    return jax.shard_map(
        shards, mesh=finer, in_specs=placed, out_specs=(P(EP, "tp"), P(EP, "tp"), P(EP, "tp")), check_vma=False
    )
```

time: 186 us -> 73.9 us (0.40)
  Pallas kernels: 0 us -> 62.3 us
  blocking collectives: 43.5 us -> 0 us
  waiting for transfers between devices: 43.2 us -> 0 us
  starting transfers between devices: 37.4 us -> 0 us
  matrix products: 17.5 us -> 0 us
  between operations: 15.1 us -> 0.64 us
  other arithmetic: 11.6 us -> 0 us
  local copies, waits for them, and re-layouts: 16.9 us -> 10.6 us
    pallas_call x0 -> x1, Pallas kernels: none -> 62.3 us  [shards(): pl.pallas_call(kernel, out_shape=(jax.ShapeDtypeStruct((ROWS, HALF), BF16...]
    all_to_all x3 -> x0, starting transfers between devices: 37.4 us -> none  [the longest x1 18.1 us: grouped_exchange(): lax.all_to_all(group, axis, split_axis=split_dim, concat_axis=concat_dim,...]
    all_gather x2 -> x0, waiting for transfers between devices: 24 us -> none  [the longest x1 24 us: gather_axes(): x = lax.all_gather(x, axis, axis=dim, tiled=True)]
    all_to_all x3 -> x0, blocking collectives: 22.7 us -> none  [the longest x2 13.7 us: sum_at_owner(): parts = lax.all_to_all(cut_along(x, dim, size), axis, 0, 0, tiled=True)]
    all_gather x2 -> x0, blocking collectives: 20.8 us -> none  [gather_axes(): x = lax.all_gather(x, axis, axis=dim, tiled=True)]
    all_to_all x3 -> x0, waiting for transfers between devices: 19.1 us -> none  [the longest x1 19.1 us: run_halves(): return lax.all_to_all(summed, EP, split_axis=1, concat_axis=1, tiled=True)]
    dot_general x12 -> x0, matrix products: 17.5 us -> none  [the longest x1 3.81 us: expert_math(): jnp.einsum('njcf,jfd->njcd', hidden, w_expert_down, preferred_element_typ...]
    reshape x6 -> x0, local copies, waits for them, and re-layouts: 6.2 us -> none  [the longest x1 2.43 us: run_halves(): summed.reshape(core_count, source_count * local_experts, item_count, summ...]
  transfers between devices with their start and end apart: 5 -> 0, of which waited for: 2 -> 0; matrix products, arithmetic and copies ran while one was open for 22% -> 0% of each run, Pallas kernels for 0% -> 0%
where the time goes in v1:
time: 73.9 us; the launch traced here: 73.6 us
  Pallas kernels  62.3 us (84%)
  local copies, waits for them, and re-layouts  10.6 us (14%)
    pallas_call x1, Pallas kernels, shards(): pl.pallas_call(kernel, out_shape=(jax.ShapeDtypeStruct((ROWS, HALF), BF16...  62.3 us
    unnamed x7, local copies, waits for them, and re-layouts  10.6 us

profile of v1, /device:TPU:1, one launch (start us, length us, event | category | flops | bytes accessed | tf_op | source)
XLA Modules:
  0.0 73.6 jit_solution(3251817113813328710)
XLA Ops:
  0.6 1.4 %copy.25.routes_h = s32[16,6]{1,0:T(8,128)} copy(s32[16,6]{0,1:T(8,128)} %param.32) | data formatting | bytes 768 | tf_op args[12]
  2.0 1.4 %copy.26.wdd_h = bf16[256,16]{1,0:T(8,128)(2,1)} copy(bf16[256,16]{0,1:T(8,128)(2,1)} %param.35) | data formatting | bytes 16384 | tf_op args[15]
  3.4 1.9 %copy.23.wk_h = bf16[2048,64]{1,0:T(8,128)(2,1)} copy(bf16[2048,64]{0,1:T(8,128)(2,1)} %param.24) | data formatting | bytes 524288 | tf_op args[4]
  5.4 2.0 %copy.24.wv_h = bf16[2048,64]{1,0:T(8,128)(2,1)} copy(bf16[2048,64]{0,1:T(8,128)(2,1)} %param.25) | data formatting | bytes 524288 | tf_op args[5]
  7.3 62.3 %shard_map.211 = (bf16[16,1024]{1,0:T(8,128)(2,1)}, bf16[16,64]{1,0:T(8,128)(2,1)}, bf16[16,64]{1,0:T(8,128)(2,1)}) custom-call(bf16[16,2048]{1,0:T(8,128)(2,1)} %tokens_h.1, s32[16]{0:T(128)} %lengths.1, f32[1,2048]{1,0:T(1,128)} %bitcast.13, bf16[2048,512]{1,0:T(8,128)(2,1)} %wq_h.1, bf16[2048,64]{1,0:T(8,128)(2,1)} %copy.23.wk_h, ...), custom_call_target="tpu_custom_call" | custom-call | tf_op jit(solution)/shard_map/pallas_call | solution.py:366
  69.7 1.4 %copy.30 = bf16[16,1024]{1,0:T(8,128)(2,1)} copy(bf16[16,1024]{1,0:T(8,128)(2,1)} %get-tuple-element.6) | data formatting | bytes 65536
  71.0 1.3 %copy.31 = bf16[16,64]{1,0:T(8,128)(2,1)} copy(bf16[16,64]{1,0:T(8,128)(2,1)} %get-tuple-element.7) | data formatting | bytes 4096
  72.3 1.3 %copy.32 = bf16[16,64]{1,0:T(8,128)(2,1)} copy(bf16[16,64]{1,0:T(8,128)(2,1)} %get-tuple-element.8) | data formatting | bytes 4096

commit v2 on v1

--- a/solution.py
+++ b/solution.py
@@ -57,6 +57,16 @@
     load_sem, w3z_s, w3z_r, w3x_s, w3x_r, w3y_s, w3y_r, h_s, h_r, ap_s, ap_r, tz_s, tz_r, g_s, g_r,
     tf_s, tf_r, xs_s, xs_r, xf_s, xf_r, eo_s, eo_r, ys_s, ys_r, dn_s, dn_r, ps_s, ps_r,
 ):
+    scope = []
+
+    def stage(name=None):
+        if scope:
+            scope.pop().__exit__(None, None, None)
+        if name:
+            scope.append(jax.named_scope(name))
+            scope[0].__enter__()
+
+    stage("enter")
     z, y, x, t = (lax.axis_index(a) for a in ("z", "y", "x", "tp"))
 
     def at_z(dz):
@@ -105,27 +115,29 @@
     ld_eg = [load(weg_h, weg), load(weu_h, weu)]
     ld_ed = [load(wed_h.at[:, pl.ds(h * HALF, HALF)], wed.at[h]) for h in range(2)]
 
+    stage("dense_slices")
     for copy in ld_dense:
         copy.wait()
     lane = iota((1, NZ * 128), 1)
     first = lax.rem(z + lane // 128, NZ) * 32
     within = lane % 128
     unit = iota((256, NZ * 128), 0)
-    eye = bits(iota((ROWS, ROWS), 0) == iota((ROWS, ROWS), 1))
-    down_t = dot_nt(eye, wdd[...]).astype(BF16)
     pieces = jnp.zeros((ROWS, NZ * 128), F32)
-    for k, w in enumerate((wdg[...], wdu[...], down_t)):
+    for k, w in enumerate((wdg[...], wdu[...], wdd[...])):
         target = jnp.where((within >= 32 * k) & (within < 32 * k + 32), first + within - 32 * k, -1)
         pieces = pieces + dot(w, bits(unit == target))
     pieces = pieces.astype(BF16)
     for dz in range(NZ):
         w3p[dz] = pieces[:, dz * 128 : (dz + 1) * 128]
-    own_hits = jnp.zeros((ROWS, 128), F32)
-    for k in range(routes.shape[1]):
-        own_hits = own_hits + jnp.where(routes[:, k : k + 1] == iota((ROWS, 128), 1), 1.0, 0.0)
+    hits_t = jnp.zeros((128, ROWS), F32)
+    for k in range(routes.shape[0]):
+        hits_t = hits_t + jnp.where(routes[k : k + 1, :] == iota((128, ROWS), 0), 1.0, 0.0)
+    eye = bits(iota((ROWS, ROWS), 0) == iota((ROWS, ROWS), 1))
+    own_hits = dot_nt(eye, hits_t.astype(BF16))
     hits[0] = own_hits.astype(BF16)
     w3[z, y, x] = w3p[0]
 
+    stage("project")
     for copy in ld_tok:
         copy.wait()
     normed = rms_scale(tokens[...], attn_gain[...])
@@ -133,9 +145,10 @@
     queries = dot(normed, wq[...]).astype(BF16)
     for copy in ld_kv:
         copy.wait()
-    new_keys[...] = dot(normed, wk[...]).astype(BF16)
-    new_values[...] = dot(normed, wv[...]).astype(BF16)
-
+    new_keys[...] = dot_nt(normed, wk[...]).astype(BF16)
+    new_values[...] = dot_nt(normed, wv[...]).astype(BF16)
+
+    stage("barrier")
     pl.semaphore_wait(barrier, len(others))
     w3z = [remote(w3p.at[d], w3.at[z, y, x], w3z_s.at[d], w3z_r.at[d], at_z(d)) for d in range(1, NZ)]
     hz = [remote(hits.at[0], hits.at[d], h_s.at[d], h_r.at[d], at_z(d)) for d in range(1, NZ)]
@@ -144,6 +157,7 @@
     w3x = [remote(w3.at[:, y, x], w3.at[:, y, x], w3x_s.at[d], w3x_r.at[d], at_x(d)) for d in range(1, NX)]
     w3y = [remote(w3.at[:, y], w3.at[:, y], w3y_s.at[d], w3y_r.at[d], at_y(d)) for d in range(1, NY)]
 
+    stage("attention")
     row = iota((128, 1), 0)
     rep = bits(iota((128, ROWS), 0) // 8 == iota((128, ROWS), 1))
     head_lane = iota((128, 512), 1) // 64 == iota((128, 512), 0) % 8
@@ -194,11 +208,13 @@
     by_head = jnp.where(head_lane, dot(mixed, unfold), 0.0).astype(BF16)
     gather_rows = bits(iota((ROWS, 128), 1) // 8 == iota((ROWS, 128), 0))
     heads_out = dot(gather_rows, by_head).astype(BF16)
+    stage("attention_out")
     ld_wo.wait()
     part[...] = dot(heads_out, wo[...]).astype(BF16)
     ap = remote(part, peer_part, ap_s.at[0], ap_r.at[0], partner)
     ap.start()
 
+    stage("slots")
     for copy in hz:
         copy.wait_recv()
     hit = hits[...].reshape(128, 128)
@@ -222,6 +238,7 @@
     cr, cc = iota((128, 256), 0), iota((128, 256), 1)
     taken = (tok_rank == ((cc // 8) % 2).astype(F32)) & (cr // 16 == cc % 8) & (tok_hit > 0.5)
 
+    stage("core_sum")
     for copy in ld_n2:
         copy.wait()
     ap.wait_recv()
@@ -234,6 +251,7 @@
     tz = [remote(norm2.at[t], tokf.at[t, d], tz_s.at[d], tz_r.at[d], at_z(d)) for d in range(1, NZ)]
     for d in (4, 3, 5, 2, 6, 1, 7):
         tz[d - 1].start()
+    stage("router")
     probs = sigmoid(dot(normed2, wr[...]))
     picked = own_hits * probs
     gates = picked / jnp.sum(picked, axis=-1, keepdims=True) * 2.5
@@ -243,8 +261,10 @@
     for copy in gz:
         copy.start()
 
+    stage("z_gather")
     for copy in tz:
         copy.wait_recv()
+    stage("dispatch")
     rows = dot(dispatch, tokf[t].reshape(128, HALF)).astype(BF16).reshape(PLANE, 16, HALF)
     for d in range(1, PLANE):
         xs[d] = rows[d]
@@ -258,6 +278,7 @@
     xf = [remote(xin.at[t, d], xin.at[t, d], xf_s.at[d], xf_r.at[d], partner) for d in range(PLANE)]
     xf[0].start()
 
+    stage("dense")
     for copy in w3y:
         copy.wait_recv()
     tf.wait_recv()
@@ -271,16 +292,20 @@
     dn.start()
     dn_mine[...] = dot_nt(dense_hidden, w3[pl.ds(4 * t, 4)].reshape(HALF, 128)).astype(BF16)
 
+    stage("plane_in")
     for d in reversed(order):
         xd[d - 1].wait_recv()
         xf[d].start()
     for copy in ld_eg:
         copy.wait()
+    stage("expert_own")
     mine = xin[t].reshape(256, HALF)
     gate_mine = dot(mine, weg[t])
     up_mine = dot(mine, weu[t])
+    stage("forward_wait")
     for copy in xf:
         copy.wait_recv()
+    stage("expert")
     theirs = xin[1 - t].reshape(256, HALF)
     gate_rows = gate_mine + dot(theirs, weg[1 - t])
     up_rows = up_mine + dot(theirs, weu[1 - t])
@@ -292,6 +317,7 @@
     eo.start()
     eo_mine[...] = dot(hidden, wed[t]).astype(BF16)
 
+    stage("gates")
     for copy in gz:
         copy.wait_recv()
     gmv = gm[...].reshape(128, 256)
@@ -301,16 +327,20 @@
     dn.wait_recv()
     dense = gmv[:, 128:129] * (dn_mine[...].astype(F32) + dn_peer[...].astype(F32))
 
+    stage("expert_sum")
     eo.wait_recv()
     done = (eo_mine[...].astype(F32) + eo_peer[...].astype(F32)).astype(BF16).reshape(PLANE, 16, HALF)
     for d in range(1, PLANE):
         ys[d] = done[d]
     yr[0] = done[0]
+    stage("plane_send")
     yd = [remote(ys.at[d], yr.at[d], ys_s.at[d], ys_r.at[d], back_in_plane(d)) for d in range(1, PLANE)]
     for d in order:
         yd[d - 1].start()
+    stage("plane_back")
     for copy in yd:
         copy.wait_recv()
+    stage("combine")
     back = yr[...].reshape(256, HALF)
     sums = dense + (dot(comb_high, back) + dot(comb_low, back))
     sums3 = sums.astype(BF16).reshape(NZ, ROWS, HALF)
@@ -321,14 +351,22 @@
     ]
     for d in (4, 3, 5, 2, 6, 1, 7):
         zd[d - 1].start()
+    stage("z_wait")
     total_out = resid[t].astype(F32) + sums[0:ROWS]
     for copy in zd:
         copy.wait_recv()
+    stage("finish")
     for d in range(1, NZ):
         total_out = total_out + pr[d].astype(F32)
     out[...] = total_out.astype(BF16)
     for copy in [*w3z, *hz, *w3x, *w3y, ap, *tz, *gz, tf, *xd, *xf, dn, eo, *yd, *zd]:
         copy.wait_send()
+    stage()
+
+
+def hand_over(*refs):
+    for k in range(3):
+        refs[3 + k][...] = refs[k][...]
 
 
 def shards(
@@ -337,19 +375,19 @@
     w_expert_gate, w_expert_up, w_expert_down,
 ):
     args = (
-        tokens, lengths, attn_gain.reshape(1, WIDTH), w_query, w_key, w_value, head_bias,
+        tokens, lengths, attn_gain.reshape(1, WIDTH), w_query, w_key.T, w_value.T, head_bias,
         key_cache.reshape(1024, 1024), value_cache.reshape(1024, 1024), w_attn_out,
-        ffn_gain.reshape(1, WIDTH), w_router, routes, w_dense_gate, w_dense_up, w_dense_down,
+        ffn_gain.reshape(1, WIDTH), w_router, routes.T, w_dense_gate, w_dense_up, w_dense_down.T,
         dense_mix.reshape(1, WIDTH), w_expert_gate.reshape(2, HALF, 256), w_expert_up.reshape(2, HALF, 256),
         w_expert_down.reshape(256, WIDTH),
     )
     smem = {1, 6}
     vm, dma = pltpu.VMEM, pltpu.SemaphoreType.DMA
     scratch = [
-        vm((ROWS, WIDTH), BF16), vm((1, WIDTH), F32), vm((WIDTH, 512), BF16), vm((WIDTH, 64), BF16),
-        vm((WIDTH, 64), BF16), vm((1024, 1024), BF16), vm((1024, 1024), BF16), vm((512, WIDTH), BF16),
-        vm((1, WIDTH), F32), vm((WIDTH, 128), BF16), vm((ROWS, 6), jnp.int32), vm((ROWS, 256), BF16),
-        vm((ROWS, 256), BF16), vm((256, ROWS), BF16), vm((1, WIDTH), F32),
+        vm((ROWS, WIDTH), BF16), vm((1, WIDTH), F32), vm((WIDTH, 512), BF16), vm((64, WIDTH), BF16),
+        vm((64, WIDTH), BF16), vm((1024, 1024), BF16), vm((1024, 1024), BF16), vm((512, WIDTH), BF16),
+        vm((1, WIDTH), F32), vm((WIDTH, 128), BF16), vm((6, ROWS), jnp.int32), vm((ROWS, 256), BF16),
+        vm((ROWS, 256), BF16), vm((ROWS, 256), BF16), vm((1, WIDTH), F32),
         vm((2, HALF, 256), BF16), vm((2, HALF, 256), BF16), vm((2, 256, HALF), BF16),
         vm((NZ, ROWS, 128), BF16), vm((NZ, NY, NX, ROWS, 128), BF16), vm((NZ, ROWS, 128), BF16),
         vm((NZ, ROWS, 256), F32), vm((ROWS, WIDTH), BF16), vm((ROWS, WIDTH), BF16),
@@ -363,7 +401,7 @@
     ]
     for n in (NZ, NX, NY, NZ, 1, NZ, NZ, 1, PLANE, PLANE, 1, PLANE, 1, NZ):
         scratch += [dma((n,)), dma((n,))]
-    return pl.pallas_call(
+    results = pl.pallas_call(
         kernel,
         out_shape=(
             jax.ShapeDtypeStruct((ROWS, HALF), BF16),
@@ -379,6 +417,13 @@
             collective_id=0, has_side_effects=True, vmem_limit_bytes=60 * 1024 * 1024
         ),
     )(*args)
+    whole = pl.BlockSpec(memory_space=pltpu.VMEM)
+    return pl.pallas_call(
+        hand_over,
+        out_shape=tuple(jax.ShapeDtypeStruct(r.shape, r.dtype) for r in results),
+        in_specs=[whole] * 3,
+        out_specs=(whole,) * 3,
+    )(*results)
 
 
 def solution(mesh):

time: 73.9 us -> 64.4 us (0.87)
  local copies, waits for them, and re-layouts: 10.6 us -> 0 us
  Pallas kernels: 62.3 us -> 63.6 us
    unnamed x7 -> x0, local copies, waits for them, and re-layouts: 10.6 us -> none
    pallas_call x0 -> x1, Pallas kernels: none -> 1.39 us  [shards(): pl.pallas_call(hand_over, out_shape=tuple((jax.ShapeDtypeStruct(r.shape,...]
where the time goes in v2:
time: 64.4 us; the launch traced here: 64.2 us
  Pallas kernels  63.6 us (99%)
  between operations  0.65 us (1%)
    pallas_call x1, Pallas kernels, shards(): pl.pallas_call(kernel, out_shape=(jax.ShapeDtypeStruct((ROWS, HALF), BF16...  62.2 us
    pallas_call x1, Pallas kernels, shards(): pl.pallas_call(hand_over, out_shape=tuple((jax.ShapeDtypeStruct(r.shape,...  1.39 us

profile of v2, /device:TPU:1, one launch (start us, length us, event | category | flops | bytes accessed | tf_op | source)
XLA Modules:
  0.0 64.2 jit_solution(16242472284257999099)
XLA Ops:
  0.6 62.2 %shard_map.211 = (bf16[16,1024]{1,0:T(8,128)(2,1)}, bf16[16,64]{1,0:T(8,128)(2,1)}, bf16[16,64]{1,0:T(8,128)(2,1)}) custom-call(bf16[16,2048]{1,0:T(8,128)(2,1)} %tokens_h.1, s32[16]{0:T(128)} %lengths.1, f32[1,2048]{1,0:T(1,128)} %bitcast.19, bf16[2048,512]{1,0:T(8,128)(2,1)} %wq_h.1, bf16[64,2048]{1,0:T(8,128)(2,1)} %bitcast.17, ...), custom_call_target="tpu_custom_call" | custom-call | tf_op jit(solution)/shard_map/pallas_call | solution.py:404
  62.8 1.4 %shard_map.212 = (bf16[16,1024]{1,0:T(8,128)(2,1)}, bf16[16,64]{1,0:T(8,128)(2,1)}, bf16[16,64]{1,0:T(8,128)(2,1)}) custom-call(bf16[16,1024]{1,0:T(8,128)(2,1)} %get-tuple-element.6.refs_0_, bf16[16,64]{1,0:T(8,128)(2,1)} %get-tuple-element.7.refs_1_, bf16[16,64]{1,0:T(8,128)(2,1)} %get-tuple-element.8.refs_2_), custom_call_target="tpu_custom_call" | custom-call | tf_op jit(solution)/shard_map/pallas_call | solution.py:421

commit v3 on v2

v3 whole, which is shorter than its diff:
```python
import jax
import jax.numpy as jnp
from jax import lax
from jax.experimental import pallas as pl
from jax.experimental.pallas import tpu as pltpu
from jax.sharding import Mesh
from jax.sharding import PartitionSpec as P

EP = ("z", "y", "x")
MESH = pl.DeviceIdType.MESH
NZ, NY, NX = 8, 4, 4
PLANE = NY * NX
ROWS, WIDTH, HALF = 16, 2048, 1024
F32, BF16 = jnp.float32, jnp.bfloat16
NT = (((1,), (1,)), ((), ()))
LOADS = 21
CHUNKS = 4
WIDE = HALF // CHUNKS
FAR_Z = (4, 3, 5, 2, 6, 1, 7)


def dot(a, b):
    return jnp.dot(a, b, preferred_element_type=F32)


def dot_nt(a, b):
    return lax.dot_general(a, b, NT, preferred_element_type=F32)


def iota(shape, dim):
    return lax.broadcasted_iota(jnp.int32, shape, dim)


def bits(mask):
    return jnp.where(mask, 1.0, 0.0).astype(BF16)


def two_terms(x):
    high = x.astype(BF16)
    return high, (x - high.astype(F32)).astype(BF16)


def sigmoid(x):
    return 1.0 / (1.0 + jnp.exp(-x))


def rms_scale(values, gain):
    wide = values.astype(F32)
    return (wide * lax.rsqrt(jnp.mean(wide * wide, axis=-1, keepdims=True) + 1e-06) * gain).astype(BF16)


def kernel(
    tokens_h, lengths, attn_gain_h, wq_h, wk_h, wv_h, head_bias, keys_h, values_h, wo_h,
    ffn_gain_h, wr_h, routes_h, wdg_h, wdu_h, wdd_h, mix_h, weg_h, weu_h, wed_h,
    out_h, new_keys_h, new_values_h, out, new_keys, new_values,
    tokens, attn_gain, wq, wk, wv, keys, values, wo, ffn_gain, wr, routes, wdg, wdu, wdd, mixw,
    weg, weu, wed,
    w3p, w3, hits, part, peer_part, norm2, resid, tokf, xs, xin, eo_mine, eo_send, eo_peer,
    ys, yr, dn_mine, dn_send, dn_peer, ps, pr,
    load_sem, store_sem, w3z_s, w3z_r, w3a_s, w3a_r, w3b_s, w3b_r, h_s, h_r, ap_s, ap_r, tz_s, tz_r,
    tf_s, tf_r, xs_s, xs_r, xf_s, xf_r, eo_s, eo_r, ys_s, ys_r, dn_s, dn_r, ps_s, ps_r,
):
    scope = []

    def stage(name=None):
        if scope:
            scope.pop().__exit__(None, None, None)
        if name:
            scope.append(jax.named_scope(name))
            scope[0].__enter__()

    stage("enter")
    z, y, x, t = (lax.axis_index(a) for a in ("z", "y", "x", "tp"))

    def at_z(dz):
        return (lax.rem(z + dz, NZ), y, x, t)

    def at_y(dy):
        return (z, lax.rem(y + dy, NY), x, t)

    def at_x(dx):
        return (z, y, lax.rem(x + dx, NX), t)

    def in_plane(d):
        return (z, lax.rem(y + d // NX, NY), lax.rem(x + d % NX, NX), t)

    def back_in_plane(d):
        return (z, lax.rem(y + NY - d // NX, NY), lax.rem(x + NX - d % NX, NX), t)

    partner = (z, y, x, 1 - t)

    def remote(src, dst, s, r, device):
        return pltpu.make_async_remote_copy(
            src_ref=src, dst_ref=dst, send_sem=s, recv_sem=r, device_id=device, device_id_type=MESH
        )

    def settle(like, sem):
        pltpu.make_async_copy(like, like, sem).wait()

    barrier = pltpu.get_barrier_semaphore()
    others = [at_z(d) for d in range(1, NZ)] + [in_plane(d) for d in range(1, PLANE)] + [partner]
    for device in others:
        pl.semaphore_signal(barrier, inc=1, device_id=device, device_id_type=MESH)

    loads = []

    def load(src, dst):
        copy = pltpu.make_async_copy(src, dst, load_sem.at[len(loads)])
        copy.start()
        loads.append(copy)
        return copy

    ld_dense = [load(routes_h, routes)]
    ld_tok = [load(tokens_h, tokens), load(attn_gain_h, attn_gain)]
    ld_q = load(wq_h, wq)
    ld_kv = [load(wk_h, wk), load(wv_h, wv)]
    ld_keys = load(keys_h, keys)
    ld_values = load(values_h, values)
    ld_wo = load(wo_h, wo)
    ld_dense += [load(wdg_h, wdg), load(wdu_h, wdu), load(wdd_h, wdd)]
    ld_n2 = [load(ffn_gain_h, ffn_gain), load(mix_h, mixw), load(wr_h, wr)]
    stage("project")
    for copy in ld_tok:
        copy.wait()
    normed = rms_scale(tokens[...], attn_gain[...])
    ld_q.wait()
    queries = dot(normed, wq[...]).astype(BF16)
    for copy in ld_kv:
        copy.wait()
    new_keys[...] = dot_nt(normed, wk[...]).astype(BF16)
    new_values[...] = dot_nt(normed, wv[...]).astype(BF16)
    stores = [
        pltpu.make_async_copy(new_keys, new_keys_h, store_sem.at[0]),
        pltpu.make_async_copy(new_values, new_values_h, store_sem.at[1]),
    ]
    for copy in stores:
        copy.start()

    stage("queries")
    row = iota((128, 1), 0)
    rep = bits(iota((128, ROWS), 0) // 8 == iota((128, ROWS), 1))
    head_lane = iota((128, 512), 1) // 64 == iota((128, 512), 0) % 8
    fold = bits(iota((512, 256), 0) % 64 == iota((512, 256), 1) % 64)
    own_block = iota((128, 256), 1) // 64 == (iota((128, 256), 0) // 8) % 4
    spread = jnp.where(head_lane, dot(rep, queries), 0.0).astype(BF16)
    block_q = jnp.where(own_block, dot(spread, fold), 0.0).astype(BF16)
    bias = jnp.zeros((32, 1), F32)
    for h in range(8):
        bias = jnp.where(iota((32, 1), 0) % 8 == h, head_bias[h], bias)
    after = bits(iota((256, 256), 0) > iota((256, 256), 1))
    stage("cache_wait")
    ld_keys.wait()
    ld_values.wait()
    ld_eg = [load(weg_h, weg), load(weu_h, weu)]
    ld_ed = [load(wed_h.at[:, pl.ds(h * HALF, HALF)], wed.at[h]) for h in range(2)]
    stage("attention")
    mixed = []
    for g in range(4):
        scores = dot(block_q[g * 32 : (g + 1) * 32], keys[pl.ds(g * 256, 256), :]) * 0.125 + bias
        length = jnp.zeros((32, 1), jnp.int32)
        for s in range(4):
            length = jnp.where(iota((32, 1), 0) // 8 == s, lengths[g * 4 + s], length)
        visible = iota((32, 1024), 1) < length
        soft = jnp.log1p(jnp.exp(-jnp.abs(scores)))
        log_take = jnp.minimum(scores, 0.0) - soft
        log_keep = jnp.where(visible, jnp.minimum(-scores, 0.0) - soft, 0.0)
        tiles = jnp.concatenate([log_keep[:, j * 256 : (j + 1) * 256] for j in range(4)], axis=0)
        high, low = two_terms(tiles)
        summed = dot(high, after) + dot(low, after)
        total = summed[:, 0:1] + tiles[:, 0:1]
        later = jnp.zeros((32, 1), F32)
        spans = [None] * 4
        for j in reversed(range(4)):
            spans[j] = summed[j * 32 : (j + 1) * 32] + later
            later = later + total[j * 32 : (j + 1) * 32]
        log_after = jnp.concatenate(spans, axis=1)
        stick = jnp.where(visible, jnp.exp(log_take + log_after), 0.0).astype(BF16)
        mixed.append(dot_nt(stick, values[pl.ds(g * 256, 256), :]))
    mixed = jnp.where(own_block, jnp.concatenate(mixed, axis=0), 0.0).astype(BF16)
    unfold = bits(iota((256, 512), 0) % 64 == iota((256, 512), 1) % 64)
    by_head = jnp.where(head_lane, dot(mixed, unfold), 0.0).astype(BF16)
    gather_rows = bits(iota((ROWS, 128), 1) // 8 == iota((ROWS, 128), 0))
    heads_out = dot(gather_rows, by_head).astype(BF16)
    stage("attention_out")
    ld_dense[0].wait()
    hits_t = jnp.zeros((128, ROWS), F32)
    for k in range(routes.shape[0]):
        hits_t = hits_t + jnp.where(routes[k : k + 1, :] == iota((128, ROWS), 0), 1.0, 0.0)
    eye = bits(iota((ROWS, ROWS), 0) == iota((ROWS, ROWS), 1))
    own_hits = dot_nt(eye, hits_t.astype(BF16))
    hits[0] = own_hits.astype(BF16)
    ld_wo.wait()
    part[...] = dot(heads_out, wo[...]).astype(BF16)
    ap = remote(part, peer_part, ap_s.at[0], ap_r.at[0], partner)
    stage("barrier")
    pl.semaphore_wait(barrier, len(others))
    hz = [remote(hits.at[0], hits.at[d], h_s.at[0], h_r.at[0], at_z(d)) for d in range(1, NZ)]
    ap.start()
    for copy in hz:
        copy.start()
    stage("dense_slices")
    for copy in ld_dense[1:]:
        copy.wait()
    lane = iota((1, NZ * 128), 1)
    first = lax.rem(z + lane // 128, NZ) * 32
    within = lane % 128
    unit = iota((256, NZ * 128), 0)
    pieces = jnp.zeros((ROWS, NZ * 128), F32)
    for k, w in enumerate((wdg[...], wdu[...], wdd[...])):
        target = jnp.where((within >= 32 * k) & (within < 32 * k + 32), first + within - 32 * k, -1)
        pieces = pieces + dot(w, bits(unit == target))
    pieces = pieces.astype(BF16)
    for dz in range(NZ):
        w3p[dz] = pieces[:, dz * 128 : (dz + 1) * 128]
    w3[z, y, x] = w3p[0]

    w3z = [remote(w3p.at[d], w3.at[z, y, x], w3z_s.at[0], w3z_r.at[0], at_z(d)) for d in range(1, NZ)]
    for copy in w3z:
        copy.start()
    first_hop, second_hop = [], []
    for h in range(2):
        zs = pl.ds(4 * h, 4)
        ends = [w3.at[zs, y, x]] * 3, [w3.at[zs, y] if h == 0 else w3.at[zs, :, x]] * 3
        for k, hops in enumerate((first_hop, second_hop)):
            for d in range(1, 4):
                sems = (w3a_s, w3a_r) if k == 0 else (w3b_s, w3b_r)
                to = at_x(d) if h == k else at_y(d)
                hops.append(remote(ends[k][0], ends[k][0], sems[0].at[0], sems[1].at[0], to))


    stage("core_sum")
    for copy in ld_n2:
        copy.wait()
    ap.wait_recv()
    residual = (tokens[...].astype(F32) + (part[...].astype(F32) + peer_part[...].astype(F32))).astype(BF16)
    normed2 = rms_scale(residual, ffn_gain[...])
    for h in range(2):
        resid[h] = residual[:, h * HALF : (h + 1) * HALF]
        for c in range(CHUNKS):
            norm2[h, c] = normed2[:, h * HALF + c * WIDE : h * HALF + (c + 1) * WIDE]
    for c in range(CHUNKS):
        tokf[t, c, 0] = norm2[t, c]
        for d in FAR_Z:
            remote(norm2.at[t, c], tokf.at[t, c, d], tz_s.at[0], tz_r.at[c], at_z(d)).start()
    stage("slots")
    settle(hits.at[pl.ds(1, NZ - 1)], h_r.at[0])
    hit = hits[...].reshape(128, 128)
    base = z * PLANE

    def expert_of(slot):
        d = slot // 16
        return base + lax.rem(y + d // NX, NY) * NX + lax.rem(x + d % NX, NX)

    sel = bits(iota((256, 128), 1) == expert_of(iota((256, 128), 0)))
    tok_r, tok_c = iota((128, 128), 0), iota((128, 128), 1)
    earlier_c = bits((tok_r < tok_c) & (tok_r // 16 == tok_c // 16))
    earlier_r = bits((tok_c < tok_r) & (tok_r // 16 == tok_c // 16))
    slot_hit = dot_nt(sel, hit)
    slot_rank = dot(slot_hit.astype(BF16), earlier_c)
    sr, sc = iota((256, 128), 0), iota((256, 128), 1)
    fits = (slot_rank == ((sr // 8) % 2).astype(F32)) & (sc // 16 == sr % 8)
    dispatch = jnp.where(fits, slot_hit, 0.0).astype(BF16)
    tok_hit = dot_nt(hit, sel)
    tok_rank = dot_nt(dot(earlier_r, hit).astype(BF16), sel)
    cr, cc = iota((128, 256), 0), iota((128, 256), 1)
    taken = (tok_rank == ((cc // 8) % 2).astype(F32)) & (cr // 16 == cc % 8) & (tok_hit > 0.5)

    order = sorted(range(1, PLANE), key=lambda d: -(min(d // NX, NY - d // NX) + min(d % NX, NX - d % NX)))

    def exchange(c, source, target, s_sem, r_sem, where):
        for d in order:
            remote(source.at[c, d], target.at[c, d], s_sem.at[0], r_sem(c, d), where(d)).start()

    def rows_of(ref):
        return ref[...].reshape(-1, WIDE)

    stage("w3z_wait")
    settle(w3p.at[pl.ds(1, NZ - 1)], w3z_r.at[0])
    for copy in first_hop:
        copy.start()
    tf = []
    for c in range(CHUNKS):
        stage("z_gather")
        settle(tokf.at[t, c, pl.ds(1, NZ - 1)], tz_r.at[c])
        stage("dispatch")
        rows = dot(dispatch, rows_of(tokf.at[t, c])).astype(BF16).reshape(PLANE, 16, WIDE)
        for d in range(1, PLANE):
            xs[c, d] = rows[d]
        xin[t, c, 0] = rows[0]
        exchange(c, xs, xin.at[t], xs_s, lambda c, d: xs_r.at[c, d // 4], in_plane)
        tf.append(remote(tokf.at[t, c], tokf.at[t, c], tf_s.at[c], tf_r.at[c], partner))
        tf[c].start()

    stage("plane_hop")
    settle(w3.at[:, pl.ds(0, 3), 0], w3a_r.at[0])
    for copy in second_hop:
        copy.start()
    xf = []
    gate_rows = jnp.zeros((256, 256), F32)
    up_rows = jnp.zeros((256, 256), F32)
    for c in range(CHUNKS):
        stage("plane_in")
        xf.append([])
        for r in range(NY):
            settle(xin.at[t, c, pl.ds(max(1, 4 * r), 3 + (r > 0))], xs_r.at[c, r])
            block = xin.at[t, c, pl.ds(4 * r, 4)]
            xf[c].append(remote(block, block, xf_s.at[0], xf_r.at[c, r], partner))
            xf[c][r].start()
        if c == 0:
            for copy in ld_eg:
                copy.wait()
        stage("expert_own")
        mine, part_w = rows_of(xin.at[t, c]), pl.ds(c * WIDE, WIDE)
        gate_rows = gate_rows + dot(mine, weg[t, part_w])
        up_rows = up_rows + dot(mine, weu[t, part_w])
    for c in range(CHUNKS):
        stage("forward_wait")
        for copy in xf[c]:
            copy.wait_recv()
        stage("expert")
        theirs, part_w = rows_of(xin.at[1 - t, c]), pl.ds(c * WIDE, WIDE)
        gate_rows = gate_rows + dot(theirs, weg[1 - t, part_w])
        up_rows = up_rows + dot(theirs, weu[1 - t, part_w])
    hidden = (gate_rows * sigmoid(gate_rows) * up_rows).astype(BF16)
    for copy in ld_ed:
        copy.wait()
    eo = []
    for c in range(CHUNKS):
        eo_send[c] = dot(hidden, wed[1 - t, :, c * WIDE : (c + 1) * WIDE]).astype(BF16)
        eo.append(remote(eo_send.at[c], eo_peer.at[c], eo_s.at[c], eo_r.at[c], partner))
        eo[c].start()
    for c in range(CHUNKS):
        eo_mine[c] = dot(hidden, wed[t, :, c * WIDE : (c + 1) * WIDE]).astype(BF16)

    for c in range(CHUNKS):
        stage("expert_sum")
        eo[c].wait_recv()
        done = (eo_mine[c].astype(F32) + eo_peer[c].astype(F32)).astype(BF16).reshape(PLANE, 16, WIDE)
        for d in range(1, PLANE):
            ys[c, d] = done[d]
        yr[c, 0] = done[0]
        stage("plane_send")
        exchange(c, ys, yr, ys_s, lambda c, d: ys_r.at[c], back_in_plane)

    stage("dense")
    settle(w3.at[:, pl.ds(0, 3)], w3b_r.at[0])
    pre = jnp.zeros((128, 128), F32)
    zs = WIDE // 256
    for c in range(CHUNKS):
        tf[c].wait_recv()
        for h in range(2):
            pre = pre + dot(rows_of(tokf.at[h, c]), w3[4 * h + zs * c : 4 * h + zs * (c + 1)].reshape(WIDE, 128))
    logits = jnp.zeros((128, 128), F32)
    mix = jnp.zeros((128, 1), F32)
    for c in range(CHUNKS):
        for h in range(2):
            cols = pl.ds(h * HALF + c * WIDE, WIDE)
            block = rows_of(tokf.at[h, c])
            logits = logits + dot(block, wr[cols])
            mix = mix + jnp.sum(block.astype(F32) * mixw[:, cols], axis=-1, keepdims=True)
    mix = sigmoid(mix)
    picked = hit.astype(F32) * sigmoid(logits)
    gates = picked / jnp.sum(picked, axis=-1, keepdims=True) * 2.5
    gate_high, gate_low = two_terms(gates)
    slot_gate = jnp.where(taken, dot_nt(gate_high, sel) + dot_nt(gate_low, sel), 0.0)
    comb_high, comb_low = two_terms(slot_gate)
    gate_in, up_in = pltpu.roll(pre, 64, 1), pltpu.roll(pre, 32, 1)
    used = (iota((128, 128), 1) >= 64) & (iota((128, 128), 1) < 96)
    dense_hidden = jnp.where(used, gate_in * sigmoid(gate_in) * up_in, 0.0).astype(BF16)
    dn_send[...] = dot_nt(dense_hidden, w3[pl.ds(4 * (1 - t), 4)].reshape(HALF, 128)).astype(BF16)
    dn = remote(dn_send, dn_peer, dn_s.at[0], dn_r.at[0], partner)
    dn.start()
    dn_mine[...] = dot_nt(dense_hidden, w3[pl.ds(4 * t, 4)].reshape(HALF, 128)).astype(BF16)

    stage("dense_sum")
    dn.wait_recv()
    dense = mix * (dn_mine[...].astype(F32) + dn_peer[...].astype(F32))
    own = []
    for c in range(CHUNKS):
        stage("plane_back")
        settle(yr.at[c, pl.ds(1, PLANE - 1)], ys_r.at[c])
        stage("combine")
        back = rows_of(yr.at[c])
        sums = dense[:, c * WIDE : (c + 1) * WIDE] + (dot(comb_high, back) + dot(comb_low, back))
        own.append(sums[0:ROWS])
        sums = sums.astype(BF16).reshape(NZ, ROWS, WIDE)
        for d in range(1, NZ):
            ps[c, d] = sums[d]
        for d in FAR_Z:
            remote(ps.at[c, d], pr.at[c, d], ps_s.at[0], ps_r.at[c], at_z(NZ - d)).start()
    for c in range(CHUNKS):
        stage("z_wait")
        settle(pr.at[c, pl.ds(1, NZ - 1)], ps_r.at[c])
        stage("finish")
        total_out = resid[t, :, c * WIDE : (c + 1) * WIDE].astype(F32) + own[c]
        for d in range(1, NZ):
            total_out = total_out + pr[c, d].astype(F32)
        out[c] = total_out.astype(BF16)
        stores.append(
            pltpu.make_async_copy(out.at[c], out_h.at[:, pl.ds(c * WIDE, WIDE)], store_sem.at[2 + c])
        )
        stores[-1].start()
    settle(w3p.at[pl.ds(1, NZ - 1)], w3z_s.at[0])
    settle(hits.at[pl.ds(1, NZ - 1)], h_s.at[0])
    settle(w3.at[:, pl.ds(0, 3), 0], w3a_s.at[0])
    settle(w3.at[:, pl.ds(0, 3)], w3b_s.at[0])
    settle(tokf.at[t, :, pl.ds(1, NZ - 1)], tz_s.at[0])
    settle(xs.at[:, pl.ds(1, PLANE - 1)], xs_s.at[0])
    settle(xin.at[t], xf_s.at[0])
    settle(ys.at[:, pl.ds(1, PLANE - 1)], ys_s.at[0])
    settle(ps.at[:, pl.ds(1, NZ - 1)], ps_s.at[0])
    for copy in [ap, *tf, dn, *eo]:
        copy.wait_send()
    for copy in stores:
        copy.wait()
    stage()


def hand_over(*refs):
    for k in range(3):
        refs[3 + k][...] = refs[k][...]


def shards(
    tokens, lengths, attn_gain, w_query, w_key, w_value, head_bias, key_cache, value_cache, w_attn_out,
    ffn_gain, w_router, routes, w_dense_gate, w_dense_up, w_dense_down, dense_mix,
    w_expert_gate, w_expert_up, w_expert_down,
):
    args = (
        tokens, lengths, attn_gain.reshape(1, WIDTH), w_query, w_key.T, w_value.T, head_bias,
        key_cache.reshape(1024, 1024), value_cache.reshape(1024, 1024), w_attn_out,
        ffn_gain.reshape(1, WIDTH), w_router, routes.T, w_dense_gate, w_dense_up, w_dense_down.T,
        dense_mix.reshape(1, WIDTH), w_expert_gate.reshape(2, HALF, 256), w_expert_up.reshape(2, HALF, 256),
        w_expert_down.reshape(256, WIDTH),
    )
    smem = {1, 6}
    vm, dma = pltpu.VMEM, pltpu.SemaphoreType.DMA
    scratch = [
        vm((CHUNKS, ROWS, WIDE), BF16), vm((ROWS, 64), BF16), vm((ROWS, 64), BF16),
        vm((ROWS, WIDTH), BF16), vm((1, WIDTH), F32), vm((WIDTH, 512), BF16), vm((64, WIDTH), BF16),
        vm((64, WIDTH), BF16), vm((1024, 1024), BF16), vm((1024, 1024), BF16), vm((512, WIDTH), BF16),
        vm((1, WIDTH), F32), vm((WIDTH, 128), BF16), vm((6, ROWS), jnp.int32), vm((ROWS, 256), BF16),
        vm((ROWS, 256), BF16), vm((ROWS, 256), BF16), vm((1, WIDTH), F32),
        vm((2, HALF, 256), BF16), vm((2, HALF, 256), BF16), vm((2, 256, HALF), BF16),
        vm((NZ, ROWS, 128), BF16), vm((NZ, NY, NX, ROWS, 128), BF16), vm((NZ, ROWS, 128), BF16),
        vm((ROWS, WIDTH), BF16), vm((ROWS, WIDTH), BF16),
        vm((2, CHUNKS, ROWS, WIDE), BF16), vm((2, ROWS, HALF), BF16), vm((2, CHUNKS, NZ, ROWS, WIDE), BF16),
        vm((CHUNKS, PLANE, 16, WIDE), BF16), vm((2, CHUNKS, PLANE, 16, WIDE), BF16),
        vm((CHUNKS, 256, WIDE), BF16), vm((CHUNKS, 256, WIDE), BF16), vm((CHUNKS, 256, WIDE), BF16),
        vm((CHUNKS, PLANE, 16, WIDE), BF16), vm((CHUNKS, PLANE, 16, WIDE), BF16),
        vm((128, HALF), BF16), vm((128, HALF), BF16), vm((128, HALF), BF16),
        vm((CHUNKS, NZ, ROWS, WIDE), BF16), vm((CHUNKS, NZ, ROWS, WIDE), BF16),
        dma((LOADS,)), dma((2 + CHUNKS,)),
    ]
    c = CHUNKS
    one, each, quarters = dma((1,)), dma((c,)), dma((c, NY))
    scratch += [one, one] * 5 + [one, each, each, each, one, quarters, one, quarters, each, each, one, each]
    scratch += [one, one, one, each]
    results = pl.pallas_call(
        kernel,
        out_shape=(
            jax.ShapeDtypeStruct((ROWS, HALF), BF16),
            jax.ShapeDtypeStruct((ROWS, 64), BF16),
            jax.ShapeDtypeStruct((ROWS, 64), BF16),
        ),
        in_specs=[
            pl.BlockSpec(memory_space=pltpu.SMEM if k in smem else pl.ANY) for k in range(len(args))
        ],
        out_specs=tuple(pl.BlockSpec(memory_space=pl.ANY) for _ in range(3)),
        scratch_shapes=scratch,
        compiler_params=pltpu.CompilerParams(
            collective_id=0, has_side_effects=True, vmem_limit_bytes=60 * 1024 * 1024
        ),
    )(*args)
    whole = pl.BlockSpec(memory_space=pltpu.VMEM)
    return pl.pallas_call(
        hand_over,
        out_shape=tuple(jax.ShapeDtypeStruct(r.shape, r.dtype) for r in results),
        in_specs=[whole] * 3,
        out_specs=(whole,) * 3,
    )(*results)


def solution(mesh):
    finer = Mesh(mesh.devices.reshape(NZ, NY, NX, mesh.shape["tp"]), ("z", "y", "x", "tp"))
    placed = (
        P(EP, None), P(EP), P(), P(None, "tp"), P(None, "tp"), P(None, "tp"), P("tp"),
        P(EP, "tp", None, None), P(EP, "tp", None, None), P("tp", None), P(), P(), P(EP, None),
        P(EP, "tp"), P(EP, "tp"), P("tp", EP), P(), P(EP, None, "tp"), P(EP, None, "tp"), P(EP, "tp", None),
    )
    return jax.shard_map(
        shards, mesh=finer, in_specs=placed, out_specs=(P(EP, "tp"), P(EP, "tp"), P(EP, "tp")), check_vma=False
    )
```

time: 64.4 us -> 47.2 us (0.73)
  Pallas kernels: 63.6 us -> 46.4 us
    pallas_call x1, Pallas kernels: 62.2 us -> 45 us  [shards(): pl.pallas_call(kernel, out_shape=(jax.ShapeDtypeStruct((ROWS, HALF), BF16...]
where the time goes in v3:
time: 47.2 us; the launch traced here: 47 us
  Pallas kernels  46.4 us (98%)
  between operations  0.65 us (1%)
    pallas_call x1, Pallas kernels, shards(): pl.pallas_call(kernel, out_shape=(jax.ShapeDtypeStruct((ROWS, HALF), BF16...  45 us
    pallas_call x1, Pallas kernels, shards(): pl.pallas_call(hand_over, out_shape=tuple((jax.ShapeDtypeStruct(r.shape,...  1.39 us

profile of v3, /device:TPU:1, one launch (start us, length us, event | category | flops | bytes accessed | tf_op | source)
XLA Modules:
  0.0 47.0 jit_solution(11704308919281831421)
XLA Ops:
  0.6 45.0 %shard_map.211 = (bf16[16,1024]{1,0:T(8,128)(2,1)}, bf16[16,64]{1,0:T(8,128)(2,1)}, bf16[16,64]{1,0:T(8,128)(2,1)}) custom-call(bf16[16,2048]{1,0:T(8,128)(2,1)} %tokens_h.1, s32[16]{0:T(128)} %lengths.1, f32[1,2048]{1,0:T(1,128)} %bitcast.19, bf16[2048,512]{1,0:T(8,128)(2,1)} %wq_h.1, bf16[64,2048]{1,0:T(8,128)(2,1)} %bitcast.17, ...), custom_call_target="tpu_custom_call" | custom-call | tf_op jit(solution)/shard_map/pallas_call | solution.py:459
  45.6 1.4 %shard_map.212 = (bf16[16,1024]{1,0:T(8,128)(2,1)}, bf16[16,64]{1,0:T(8,128)(2,1)}, bf16[16,64]{1,0:T(8,128)(2,1)}) custom-call(bf16[16,1024]{1,0:T(8,128)(2,1)} %get-tuple-element.6.refs_0_, bf16[16,64]{1,0:T(8,128)(2,1)} %get-tuple-element.7.refs_1_, bf16[16,64]{1,0:T(8,128)(2,1)} %get-tuple-element.8.refs_2_), custom_call_target="tpu_custom_call" | custom-call | tf_op jit(solution)/shard_map/pallas_call | solution.py:476

commit v4 on v3

--- a/solution.py
+++ b/solution.py
@@ -13,7 +13,7 @@
 ROWS, WIDTH, HALF = 16, 2048, 1024
 F32, BF16 = jnp.float32, jnp.bfloat16
 NT = (((1,), (1,)), ((), ()))
-LOADS = 21
+LOADS = 23
 CHUNKS = 4
 WIDE = HALF // CHUNKS
 FAR_Z = (4, 3, 5, 2, 6, 1, 7)
@@ -50,14 +50,14 @@
 
 
 def kernel(
-    tokens_h, lengths, attn_gain_h, wq_h, wk_h, wv_h, head_bias, keys_h, values_h, wo_h,
+    tokens_h, lengths_h, attn_gain_h, wq_h, wk_h, wv_h, head_bias_h, keys_h, values_h, wo_h,
     ffn_gain_h, wr_h, routes_h, wdg_h, wdu_h, wdd_h, mix_h, weg_h, weu_h, wed_h,
-    out_h, new_keys_h, new_values_h, out, new_keys, new_values,
-    tokens, attn_gain, wq, wk, wv, keys, values, wo, ffn_gain, wr, routes, wdg, wdu, wdd, mixw,
+    out, new_keys, new_values,
+    tokens, lengths, attn_gain, wq, wk, wv, head_bias, keys, values, wo, ffn_gain, wr, routes, wdg, wdu, wdd, mixw,
     weg, weu, wed,
     w3p, w3, hits, part, peer_part, norm2, resid, tokf, xs, xin, eo_mine, eo_send, eo_peer,
     ys, yr, dn_mine, dn_send, dn_peer, ps, pr,
-    load_sem, store_sem, w3z_s, w3z_r, w3a_s, w3a_r, w3b_s, w3b_r, h_s, h_r, ap_s, ap_r, tz_s, tz_r,
+    load_sem, w3z_s, w3z_r, w3a_s, w3a_r, w3b_s, w3b_r, h_s, h_r, ap_s, ap_r, tz_s, tz_r,
     tf_s, tf_r, xs_s, xs_r, xf_s, xf_r, eo_s, eo_r, ys_s, ys_r, dn_s, dn_r, ps_s, ps_r,
 ):
     scope = []
@@ -110,14 +110,13 @@
         loads.append(copy)
         return copy
 
-    ld_dense = [load(routes_h, routes)]
     ld_tok = [load(tokens_h, tokens), load(attn_gain_h, attn_gain)]
     ld_q = load(wq_h, wq)
+    ld_heads = [load(lengths_h, lengths), load(head_bias_h, head_bias)]
+    ld_cache = [load(keys_h, keys), load(values_h, values)]
+    ld_wo = load(wo_h, wo)
+    ld_dense = [load(routes_h, routes), load(wdg_h, wdg), load(wdu_h, wdu), load(wdd_h, wdd)]
     ld_kv = [load(wk_h, wk), load(wv_h, wv)]
-    ld_keys = load(keys_h, keys)
-    ld_values = load(values_h, values)
-    ld_wo = load(wo_h, wo)
-    ld_dense += [load(wdg_h, wdg), load(wdu_h, wdu), load(wdd_h, wdd)]
     ld_n2 = [load(ffn_gain_h, ffn_gain), load(mix_h, mixw), load(wr_h, wr)]
     stage("project")
     for copy in ld_tok:
@@ -125,17 +124,6 @@
     normed = rms_scale(tokens[...], attn_gain[...])
     ld_q.wait()
     queries = dot(normed, wq[...]).astype(BF16)
-    for copy in ld_kv:
-        copy.wait()
-    new_keys[...] = dot_nt(normed, wk[...]).astype(BF16)
-    new_values[...] = dot_nt(normed, wv[...]).astype(BF16)
-    stores = [
-        pltpu.make_async_copy(new_keys, new_keys_h, store_sem.at[0]),
-        pltpu.make_async_copy(new_values, new_values_h, store_sem.at[1]),
-    ]
-    for copy in stores:
-        copy.start()
-
     stage("queries")
     row = iota((128, 1), 0)
     rep = bits(iota((128, ROWS), 0) // 8 == iota((128, ROWS), 1))
@@ -144,15 +132,15 @@
     own_block = iota((128, 256), 1) // 64 == (iota((128, 256), 0) // 8) % 4
     spread = jnp.where(head_lane, dot(rep, queries), 0.0).astype(BF16)
     block_q = jnp.where(own_block, dot(spread, fold), 0.0).astype(BF16)
+    for copy in ld_heads:
+        copy.wait()
     bias = jnp.zeros((32, 1), F32)
     for h in range(8):
         bias = jnp.where(iota((32, 1), 0) % 8 == h, head_bias[h], bias)
     after = bits(iota((256, 256), 0) > iota((256, 256), 1))
     stage("cache_wait")
-    ld_keys.wait()
-    ld_values.wait()
-    ld_eg = [load(weg_h, weg), load(weu_h, weu)]
-    ld_ed = [load(wed_h.at[:, pl.ds(h * HALF, HALF)], wed.at[h]) for h in range(2)]
+    for copy in ld_cache:
+        copy.wait()
     stage("attention")
     mixed = []
     for g in range(4):
@@ -190,6 +178,8 @@
     own_hits = dot_nt(eye, hits_t.astype(BF16))
     hits[0] = own_hits.astype(BF16)
     ld_wo.wait()
+    ld_eg = [load(weg_h, weg), load(weu_h, weu)]
+    ld_ed = [load(wed_h.at[:, pl.ds(h * HALF, HALF)], wed.at[h]) for h in range(2)]
     part[...] = dot(heads_out, wo[...]).astype(BF16)
     ap = remote(part, peer_part, ap_s.at[0], ap_r.at[0], partner)
     stage("barrier")
@@ -213,10 +203,13 @@
     for dz in range(NZ):
         w3p[dz] = pieces[:, dz * 128 : (dz + 1) * 128]
     w3[z, y, x] = w3p[0]
+    for copy in ld_kv:
+        copy.wait()
+    new_keys[...] = dot_nt(normed, wk[...]).astype(BF16)
+    new_values[...] = dot_nt(normed, wv[...]).astype(BF16)
+
 
     w3z = [remote(w3p.at[d], w3.at[z, y, x], w3z_s.at[0], w3z_r.at[0], at_z(d)) for d in range(1, NZ)]
-    for copy in w3z:
-        copy.start()
     first_hop, second_hop = [], []
     for h in range(2):
         zs = pl.ds(4 * h, 4)
@@ -242,6 +235,9 @@
         tokf[t, c, 0] = norm2[t, c]
         for d in FAR_Z:
             remote(norm2.at[t, c], tokf.at[t, c, d], tz_s.at[0], tz_r.at[c], at_z(d)).start()
+        if c == 0:
+            for copy in w3z:
+                copy.start()
     stage("slots")
     settle(hits.at[pl.ds(1, NZ - 1)], h_r.at[0])
     hit = hits[...].reshape(128, 128)
@@ -274,10 +270,6 @@
     def rows_of(ref):
         return ref[...].reshape(-1, WIDE)
 
-    stage("w3z_wait")
-    settle(w3p.at[pl.ds(1, NZ - 1)], w3z_r.at[0])
-    for copy in first_hop:
-        copy.start()
     tf = []
     for c in range(CHUNKS):
         stage("z_gather")
@@ -290,6 +282,11 @@
         exchange(c, xs, xin.at[t], xs_s, lambda c, d: xs_r.at[c, d // 4], in_plane)
         tf.append(remote(tokf.at[t, c], tokf.at[t, c], tf_s.at[c], tf_r.at[c], partner))
         tf[c].start()
+        if c == 0:
+            stage("w3z_wait")
+            settle(w3p.at[pl.ds(1, NZ - 1)], w3z_r.at[0])
+            for copy in first_hop:
+                copy.start()
 
     stage("plane_hop")
     settle(w3.at[:, pl.ds(0, 3), 0], w3a_r.at[0])
@@ -395,11 +392,7 @@
         total_out = resid[t, :, c * WIDE : (c + 1) * WIDE].astype(F32) + own[c]
         for d in range(1, NZ):
             total_out = total_out + pr[c, d].astype(F32)
-        out[c] = total_out.astype(BF16)
-        stores.append(
-            pltpu.make_async_copy(out.at[c], out_h.at[:, pl.ds(c * WIDE, WIDE)], store_sem.at[2 + c])
-        )
-        stores[-1].start()
+        out[:, c * WIDE : (c + 1) * WIDE] = total_out.astype(BF16)
     settle(w3p.at[pl.ds(1, NZ - 1)], w3z_s.at[0])
     settle(hits.at[pl.ds(1, NZ - 1)], h_s.at[0])
     settle(w3.at[:, pl.ds(0, 3), 0], w3a_s.at[0])
@@ -411,8 +404,6 @@
     settle(ps.at[:, pl.ds(1, NZ - 1)], ps_s.at[0])
     for copy in [ap, *tf, dn, *eo]:
         copy.wait_send()
-    for copy in stores:
-        copy.wait()
     stage()
 
 
@@ -433,12 +424,10 @@
         dense_mix.reshape(1, WIDTH), w_expert_gate.reshape(2, HALF, 256), w_expert_up.reshape(2, HALF, 256),
         w_expert_down.reshape(256, WIDTH),
     )
-    smem = {1, 6}
     vm, dma = pltpu.VMEM, pltpu.SemaphoreType.DMA
     scratch = [
-        vm((CHUNKS, ROWS, WIDE), BF16), vm((ROWS, 64), BF16), vm((ROWS, 64), BF16),
-        vm((ROWS, WIDTH), BF16), vm((1, WIDTH), F32), vm((WIDTH, 512), BF16), vm((64, WIDTH), BF16),
-        vm((64, WIDTH), BF16), vm((1024, 1024), BF16), vm((1024, 1024), BF16), vm((512, WIDTH), BF16),
+        vm((ROWS, WIDTH), BF16), pltpu.SMEM((ROWS,), jnp.int32), vm((1, WIDTH), F32), vm((WIDTH, 512), BF16),
+        vm((64, WIDTH), BF16), vm((64, WIDTH), BF16), pltpu.SMEM((8,), F32), vm((1024, 1024), BF16), vm((1024, 1024), BF16), vm((512, WIDTH), BF16),
         vm((1, WIDTH), F32), vm((WIDTH, 128), BF16), vm((6, ROWS), jnp.int32), vm((ROWS, 256), BF16),
         vm((ROWS, 256), BF16), vm((ROWS, 256), BF16), vm((1, WIDTH), F32),
         vm((2, HALF, 256), BF16), vm((2, HALF, 256), BF16), vm((2, 256, HALF), BF16),
@@ -450,7 +439,7 @@
         vm((CHUNKS, PLANE, 16, WIDE), BF16), vm((CHUNKS, PLANE, 16, WIDE), BF16),
         vm((128, HALF), BF16), vm((128, HALF), BF16), vm((128, HALF), BF16),
         vm((CHUNKS, NZ, ROWS, WIDE), BF16), vm((CHUNKS, NZ, ROWS, WIDE), BF16),
-        dma((LOADS,)), dma((2 + CHUNKS,)),
+        dma((LOADS,)),
     ]
     c = CHUNKS
     one, each, quarters = dma((1,)), dma((c,)), dma((c, NY))
@@ -459,14 +448,14 @@
     results = pl.pallas_call(
         kernel,
         out_shape=(
-            jax.ShapeDtypeStruct((ROWS, HALF), BF16),
-            jax.ShapeDtypeStruct((ROWS, 64), BF16),
-            jax.ShapeDtypeStruct((ROWS, 64), BF16),
+            pltpu.VMEM((ROWS, HALF), BF16),
+            pltpu.VMEM((ROWS, 64), BF16),
+            pltpu.VMEM((ROWS, 64), BF16),
         ),
         in_specs=[
-            pl.BlockSpec(memory_space=pltpu.SMEM if k in smem else pl.ANY) for k in range(len(args))
+            pl.BlockSpec(memory_space=pl.ANY) for _ in args
         ],
-        out_specs=tuple(pl.BlockSpec(memory_space=pl.ANY) for _ in range(3)),
+        out_specs=tuple(pl.BlockSpec(memory_space=pltpu.VMEM) for _ in range(3)),
         scratch_shapes=scratch,
         compiler_params=pltpu.CompilerParams(
             collective_id=0, has_side_effects=True, vmem_limit_bytes=60 * 1024 * 1024
@@ -478,7 +467,7 @@
         out_shape=tuple(jax.ShapeDtypeStruct(r.shape, r.dtype) for r in results),
         in_specs=[whole] * 3,
         out_specs=(whole,) * 3,
-    )(*results)
+    )(*(pltpu.with_memory_space_constraint(r, pltpu.VMEM) for r in results))
 
 
 def solution(mesh):

time: 47.2 us -> 45.7 us (0.968)
  Pallas kernels: 46.4 us -> 44.9 us
    pallas_call x1, Pallas kernels: 1.39 us -> 0.63 us  [shards(): pl.pallas_call(hand_over, out_shape=tuple((jax.ShapeDtypeStruct(r.shape,...]
    pallas_call x1, Pallas kernels: 45 us -> 44.3 us  [shards(): pl.pallas_call(kernel, out_shape=(pltpu.VMEM((ROWS, HALF), BF16), pltpu.V...]
where the time goes in v4:
time: 45.7 us; the launch traced here: 45.6 us
  Pallas kernels  44.9 us (98%)
  between operations  0.65 us (1%)
    pallas_call x1, Pallas kernels, shards(): pl.pallas_call(kernel, out_shape=(pltpu.VMEM((ROWS, HALF), BF16), pltpu.V...  44.3 us

profile of v4, /device:TPU:1, one launch (start us, length us, event | category | flops | bytes accessed | tf_op | source)
XLA Modules:
  0.0 45.6 jit_solution(5959038667215537334)
XLA Ops:
  0.6 44.3 %shard_map.211 = (bf16[16,1024]{1,0:T(8,128)(2,1)S(1)}, bf16[16,64]{1,0:T(8,128)(2,1)S(1)}, bf16[16,64]{1,0:T(8,128)(2,1)S(1)}) custom-call(bf16[16,2048]{1,0:T(8,128)(2,1)} %tokens_h.1, s32[16]{0:T(128)} %lengths_h.1, f32[1,2048]{1,0:T(1,128)} %bitcast.19, bf16[2048,512]{1,0:T(8,128)(2,1)} %wq_h.1, bf16[64,2048]{1,0:T(8,128)(2,1)} %bitcast.17, ...), custom_call_target="tpu_custom_call" | custom-call | tf_op jit(solution)/shard_map/pallas_call | solution.py:448
  45.0 0.6 %shard_map.212 = (bf16[16,1024]{1,0:T(8,128)(2,1)}, bf16[16,64]{1,0:T(8,128)(2,1)}, bf16[16,64]{1,0:T(8,128)(2,1)}) custom-call(bf16[16,1024]{1,0:T(8,128)(2,1)S(1)} %get-tuple-element.6.refs_0_, bf16[16,64]{1,0:T(8,128)(2,1)S(1)} %get-tuple-element.7.refs_1_, bf16[16,64]{1,0:T(8,128)(2,1)S(1)} %get-tuple-element.8.refs_2_), custom_call_target="tpu_custom_call" | custom-call | tf_op jit(solution)/shard_map/pallas_call | solution.py:465

commit v5 on v4

--- a/solution.py
+++ b/solution.py
@@ -55,7 +55,7 @@
     out, new_keys, new_values,
     tokens, lengths, attn_gain, wq, wk, wv, head_bias, keys, values, wo, ffn_gain, wr, routes, wdg, wdu, wdd, mixw,
     weg, weu, wed,
-    w3p, w3, hits, part, peer_part, norm2, resid, tokf, xs, xin, eo_mine, eo_send, eo_peer,
+    w3p, w3, hits, part, peer_part, norm2, resid, tokf, xs, xin,
     ys, yr, dn_mine, dn_send, dn_peer, ps, pr,
     load_sem, w3z_s, w3z_r, w3a_s, w3a_r, w3b_s, w3b_r, h_s, h_r, ap_s, ap_r, tz_s, tz_r,
     tf_s, tf_r, xs_s, xs_r, xf_s, xf_r, eo_s, eo_r, ys_s, ys_r, dn_s, dn_r, ps_s, ps_r,
@@ -97,12 +97,15 @@
     def settle(like, sem):
         pltpu.make_async_copy(like, like, sem).wait()
 
-    barrier = pltpu.get_barrier_semaphore()
-    others = [at_z(d) for d in range(1, NZ)] + [in_plane(d) for d in range(1, PLANE)] + [partner]
-    for device in others:
-        pl.semaphore_signal(barrier, inc=1, device_id=device, device_id_type=MESH)
-
     loads = []
+
+    def load_split(src, dst, pieces):
+        sem = load_sem.at[len(loads)]
+        rows = src.shape[0] // pieces
+        for k in range(pieces):
+            pltpu.make_async_copy(src.at[pl.ds(k * rows, rows)], dst.at[pl.ds(k * rows, rows)], sem).start()
+        loads.append(pltpu.make_async_copy(src, dst, sem))
+        return loads[-1]
 
     def load(src, dst):
         copy = pltpu.make_async_copy(src, dst, load_sem.at[len(loads)])
@@ -110,34 +113,60 @@
         loads.append(copy)
         return copy
 
+    ld_dense = [load(routes_h, routes), load(wdg_h, wdg), load(wdu_h, wdu), load(wdd_h, wdd)]
     ld_tok = [load(tokens_h, tokens), load(attn_gain_h, attn_gain)]
     ld_q = load(wq_h, wq)
     ld_heads = [load(lengths_h, lengths), load(head_bias_h, head_bias)]
-    ld_cache = [load(keys_h, keys), load(values_h, values)]
-    ld_wo = load(wo_h, wo)
-    ld_dense = [load(routes_h, routes), load(wdg_h, wdg), load(wdu_h, wdu), load(wdd_h, wdd)]
-    ld_kv = [load(wk_h, wk), load(wv_h, wv)]
-    ld_n2 = [load(ffn_gain_h, ffn_gain), load(mix_h, mixw), load(wr_h, wr)]
+    ld_cache = [load_split(keys_h, keys, 4), load_split(values_h, values, 4)]
+    barrier = pltpu.get_barrier_semaphore()
+    others = [at_z(d) for d in range(1, NZ)] + [in_plane(d) for d in range(1, PLANE)] + [partner]
+    for device in others:
+        pl.semaphore_signal(barrier, inc=1, device_id=device, device_id_type=MESH)
+
     stage("project")
     for copy in ld_tok:
         copy.wait()
     normed = rms_scale(tokens[...], attn_gain[...])
-    ld_q.wait()
-    queries = dot(normed, wq[...]).astype(BF16)
-    stage("queries")
-    row = iota((128, 1), 0)
     rep = bits(iota((128, ROWS), 0) // 8 == iota((128, ROWS), 1))
     head_lane = iota((128, 512), 1) // 64 == iota((128, 512), 0) % 8
     fold = bits(iota((512, 256), 0) % 64 == iota((512, 256), 1) % 64)
     own_block = iota((128, 256), 1) // 64 == (iota((128, 256), 0) // 8) % 4
-    spread = jnp.where(head_lane, dot(rep, queries), 0.0).astype(BF16)
-    block_q = jnp.where(own_block, dot(spread, fold), 0.0).astype(BF16)
     for copy in ld_heads:
         copy.wait()
     bias = jnp.zeros((32, 1), F32)
     for h in range(8):
         bias = jnp.where(iota((32, 1), 0) % 8 == h, head_bias[h], bias)
     after = bits(iota((256, 256), 0) > iota((256, 256), 1))
+    ld_dense[0].wait()
+    hits_t = jnp.zeros((128, ROWS), F32)
+    for k in range(routes.shape[0]):
+        hits_t = hits_t + jnp.where(routes[k : k + 1, :] == iota((128, ROWS), 0), 1.0, 0.0)
+    eye = bits(iota((ROWS, ROWS), 0) == iota((ROWS, ROWS), 1))
+    own_hits = dot_nt(eye, hits_t.astype(BF16))
+    hits[0] = own_hits.astype(BF16)
+    for copy in ld_dense[1:]:
+        copy.wait()
+    lane = iota((1, NZ * 128), 1)
+    first = lax.rem(z + lane // 128, NZ) * 32
+    within = lane % 128
+    unit = iota((256, NZ * 128), 0)
+    pieces = jnp.zeros((ROWS, NZ * 128), F32)
+    for k, w in enumerate((wdg[...], wdu[...], wdd[...])):
+        target = jnp.where((within >= 32 * k) & (within < 32 * k + 32), first + within - 32 * k, -1)
+        pieces = pieces + dot(w, bits(unit == target))
+    pieces = pieces.astype(BF16)
+    for dz in range(NZ):
+        w3p[dz] = pieces[:, dz * 128 : (dz + 1) * 128]
+    w3[z, y, x] = w3p[0]
+    stage("query_wait")
+    ld_q.wait()
+    ld_wo = load(wo_h, wo)
+    ld_kv = [load(wk_h, wk), load(wv_h, wv)]
+    ld_n2 = [load(ffn_gain_h, ffn_gain), load(mix_h, mixw), load(wr_h, wr)]
+    queries = dot(normed, wq[...]).astype(BF16)
+    stage("queries")
+    spread = jnp.where(head_lane, dot(rep, queries), 0.0).astype(BF16)
+    block_q = jnp.where(own_block, dot(spread, fold), 0.0).astype(BF16)
     stage("cache_wait")
     for copy in ld_cache:
         copy.wait()
@@ -149,7 +178,7 @@
         for s in range(4):
             length = jnp.where(iota((32, 1), 0) // 8 == s, lengths[g * 4 + s], length)
         visible = iota((32, 1024), 1) < length
-        soft = jnp.log1p(jnp.exp(-jnp.abs(scores)))
+        soft = jnp.log(1.0 + jnp.exp(-jnp.abs(scores)))
         log_take = jnp.minimum(scores, 0.0) - soft
         log_keep = jnp.where(visible, jnp.minimum(-scores, 0.0) - soft, 0.0)
         tiles = jnp.concatenate([log_keep[:, j * 256 : (j + 1) * 256] for j in range(4)], axis=0)
@@ -170,46 +199,18 @@
     gather_rows = bits(iota((ROWS, 128), 1) // 8 == iota((ROWS, 128), 0))
     heads_out = dot(gather_rows, by_head).astype(BF16)
     stage("attention_out")
-    ld_dense[0].wait()
-    hits_t = jnp.zeros((128, ROWS), F32)
-    for k in range(routes.shape[0]):
-        hits_t = hits_t + jnp.where(routes[k : k + 1, :] == iota((128, ROWS), 0), 1.0, 0.0)
-    eye = bits(iota((ROWS, ROWS), 0) == iota((ROWS, ROWS), 1))
-    own_hits = dot_nt(eye, hits_t.astype(BF16))
-    hits[0] = own_hits.astype(BF16)
     ld_wo.wait()
-    ld_eg = [load(weg_h, weg), load(weu_h, weu)]
-    ld_ed = [load(wed_h.at[:, pl.ds(h * HALF, HALF)], wed.at[h]) for h in range(2)]
+    ld_eg = [load(weg_h, weg.at[0]), load(weu_h, weu.at[0])]
+    ld_ed = [load(wed_h.at[:, pl.ds(h * HALF, HALF)], wed.at[0, h]) for h in range(2)]
     part[...] = dot(heads_out, wo[...]).astype(BF16)
     ap = remote(part, peer_part, ap_s.at[0], ap_r.at[0], partner)
     stage("barrier")
     pl.semaphore_wait(barrier, len(others))
     hz = [remote(hits.at[0], hits.at[d], h_s.at[0], h_r.at[0], at_z(d)) for d in range(1, NZ)]
+    w3z = [remote(w3p.at[d], w3.at[z, y, x], w3z_s.at[0], w3z_r.at[0], at_z(d)) for d in range(1, NZ)]
     ap.start()
-    for copy in hz:
+    for copy in hz + w3z:
         copy.start()
-    stage("dense_slices")
-    for copy in ld_dense[1:]:
-        copy.wait()
-    lane = iota((1, NZ * 128), 1)
-    first = lax.rem(z + lane // 128, NZ) * 32
-    within = lane % 128
-    unit = iota((256, NZ * 128), 0)
-    pieces = jnp.zeros((ROWS, NZ * 128), F32)
-    for k, w in enumerate((wdg[...], wdu[...], wdd[...])):
-        target = jnp.where((within >= 32 * k) & (within < 32 * k + 32), first + within - 32 * k, -1)
-        pieces = pieces + dot(w, bits(unit == target))
-    pieces = pieces.astype(BF16)
-    for dz in range(NZ):
-        w3p[dz] = pieces[:, dz * 128 : (dz + 1) * 128]
-    w3[z, y, x] = w3p[0]
-    for copy in ld_kv:
-        copy.wait()
-    new_keys[...] = dot_nt(normed, wk[...]).astype(BF16)
-    new_values[...] = dot_nt(normed, wv[...]).astype(BF16)
-
-
-    w3z = [remote(w3p.at[d], w3.at[z, y, x], w3z_s.at[0], w3z_r.at[0], at_z(d)) for d in range(1, NZ)]
     first_hop, second_hop = [], []
     for h in range(2):
         zs = pl.ds(4 * h, 4)
@@ -235,9 +236,23 @@
         tokf[t, c, 0] = norm2[t, c]
         for d in FAR_Z:
             remote(norm2.at[t, c], tokf.at[t, c, d], tz_s.at[0], tz_r.at[c], at_z(d)).start()
-        if c == 0:
-            for copy in w3z:
-                copy.start()
+    stage("new_rows")
+    for copy in ld_kv:
+        copy.wait()
+    new_keys[...] = dot_nt(normed, wk[...]).astype(BF16)
+    new_values[...] = dot_nt(normed, wv[...]).astype(BF16)
+
+
+    stage("weights_send")
+    for copy in ld_eg:
+        copy.wait()
+    shared = [
+        remote(weg.at[0], weg.at[1], eo_s.at[0], eo_r.at[0], partner),
+        remote(weu.at[0], weu.at[1], eo_s.at[1], eo_r.at[1], partner),
+        remote(wed.at[0, 1 - t], wed.at[1, 1 - t], eo_s.at[2], eo_r.at[2], partner),
+    ]
+    shared[0].start()
+    shared[1].start()
     stage("slots")
     settle(hits.at[pl.ds(1, NZ - 1)], h_r.at[0])
     hit = hits[...].reshape(128, 128)
@@ -282,6 +297,10 @@
         exchange(c, xs, xin.at[t], xs_s, lambda c, d: xs_r.at[c, d // 4], in_plane)
         tf.append(remote(tokf.at[t, c], tokf.at[t, c], tf_s.at[c], tf_r.at[c], partner))
         tf[c].start()
+        if c == 1:
+            for copy in ld_ed:
+                copy.wait()
+            shared[2].start()
         if c == 0:
             stage("w3z_wait")
             settle(w3p.at[pl.ds(1, NZ - 1)], w3z_r.at[0])
@@ -293,8 +312,8 @@
     for copy in second_hop:
         copy.start()
     xf = []
-    gate_rows = jnp.zeros((256, 256), F32)
-    up_rows = jnp.zeros((256, 256), F32)
+    gate_rows = [jnp.zeros((256, 256), F32)] * 2
+    up_rows = [jnp.zeros((256, 256), F32)] * 2
     for c in range(CHUNKS):
         stage("plane_in")
         xf.append([])
@@ -304,35 +323,29 @@
             xf[c].append(remote(block, block, xf_s.at[0], xf_r.at[c, r], partner))
             xf[c][r].start()
         if c == 0:
-            for copy in ld_eg:
-                copy.wait()
+            shared[0].wait_recv()
+            shared[1].wait_recv()
         stage("expert_own")
         mine, part_w = rows_of(xin.at[t, c]), pl.ds(c * WIDE, WIDE)
-        gate_rows = gate_rows + dot(mine, weg[t, part_w])
-        up_rows = up_rows + dot(mine, weu[t, part_w])
+        for k in range(2):
+            gate_rows[k] = gate_rows[k] + dot(mine, weg[k, t, part_w])
+            up_rows[k] = up_rows[k] + dot(mine, weu[k, t, part_w])
     for c in range(CHUNKS):
         stage("forward_wait")
         for copy in xf[c]:
             copy.wait_recv()
         stage("expert")
         theirs, part_w = rows_of(xin.at[1 - t, c]), pl.ds(c * WIDE, WIDE)
-        gate_rows = gate_rows + dot(theirs, weg[1 - t, part_w])
-        up_rows = up_rows + dot(theirs, weu[1 - t, part_w])
-    hidden = (gate_rows * sigmoid(gate_rows) * up_rows).astype(BF16)
-    for copy in ld_ed:
-        copy.wait()
-    eo = []
-    for c in range(CHUNKS):
-        eo_send[c] = dot(hidden, wed[1 - t, :, c * WIDE : (c + 1) * WIDE]).astype(BF16)
-        eo.append(remote(eo_send.at[c], eo_peer.at[c], eo_s.at[c], eo_r.at[c], partner))
-        eo[c].start()
-    for c in range(CHUNKS):
-        eo_mine[c] = dot(hidden, wed[t, :, c * WIDE : (c + 1) * WIDE]).astype(BF16)
-
-    for c in range(CHUNKS):
-        stage("expert_sum")
-        eo[c].wait_recv()
-        done = (eo_mine[c].astype(F32) + eo_peer[c].astype(F32)).astype(BF16).reshape(PLANE, 16, WIDE)
+        for k in range(2):
+            gate_rows[k] = gate_rows[k] + dot(theirs, weg[k, 1 - t, part_w])
+            up_rows[k] = up_rows[k] + dot(theirs, weu[k, 1 - t, part_w])
+    hidden = [(gate_rows[k] * sigmoid(gate_rows[k]) * up_rows[k]).astype(BF16) for k in range(2)]
+    shared[2].wait_recv()
+    for c in range(CHUNKS):
+        stage("expert_out")
+        cols = pl.ds(c * WIDE, WIDE)
+        done = dot(hidden[0], wed[0, t, :, cols]) + dot(hidden[1], wed[1, t, :, cols])
+        done = done.astype(BF16).reshape(PLANE, 16, WIDE)
         for d in range(1, PLANE):
             ys[c, d] = done[d]
         yr[c, 0] = done[0]
@@ -402,7 +415,7 @@
     settle(xin.at[t], xf_s.at[0])
     settle(ys.at[:, pl.ds(1, PLANE - 1)], ys_s.at[0])
     settle(ps.at[:, pl.ds(1, NZ - 1)], ps_s.at[0])
-    for copy in [ap, *tf, dn, *eo]:
+    for copy in [ap, *tf, dn, *shared]:
         copy.wait_send()
     stage()
 
@@ -430,12 +443,11 @@
         vm((64, WIDTH), BF16), vm((64, WIDTH), BF16), pltpu.SMEM((8,), F32), vm((1024, 1024), BF16), vm((1024, 1024), BF16), vm((512, WIDTH), BF16),
         vm((1, WIDTH), F32), vm((WIDTH, 128), BF16), vm((6, ROWS), jnp.int32), vm((ROWS, 256), BF16),
         vm((ROWS, 256), BF16), vm((ROWS, 256), BF16), vm((1, WIDTH), F32),
-        vm((2, HALF, 256), BF16), vm((2, HALF, 256), BF16), vm((2, 256, HALF), BF16),
+        vm((2, 2, HALF, 256), BF16), vm((2, 2, HALF, 256), BF16), vm((2, 2, 256, HALF), BF16),
         vm((NZ, ROWS, 128), BF16), vm((NZ, NY, NX, ROWS, 128), BF16), vm((NZ, ROWS, 128), BF16),
         vm((ROWS, WIDTH), BF16), vm((ROWS, WIDTH), BF16),
         vm((2, CHUNKS, ROWS, WIDE), BF16), vm((2, ROWS, HALF), BF16), vm((2, CHUNKS, NZ, ROWS, WIDE), BF16),
         vm((CHUNKS, PLANE, 16, WIDE), BF16), vm((2, CHUNKS, PLANE, 16, WIDE), BF16),
-        vm((CHUNKS, 256, WIDE), BF16), vm((CHUNKS, 256, WIDE), BF16), vm((CHUNKS, 256, WIDE), BF16),
         vm((CHUNKS, PLANE, 16, WIDE), BF16), vm((CHUNKS, PLANE, 16, WIDE), BF16),
         vm((128, HALF), BF16), vm((128, HALF), BF16), vm((128, HALF), BF16),
         vm((CHUNKS, NZ, ROWS, WIDE), BF16), vm((CHUNKS, NZ, ROWS, WIDE), BF16),

time: 45.7 us -> 44.7 us (0.978)
  Pallas kernels: 44.9 us -> 44 us
    pallas_call x1, Pallas kernels: 44.3 us -> 43.4 us  [shards(): pl.pallas_call(kernel, out_shape=(pltpu.VMEM((ROWS, HALF), BF16), pltpu.V...]
where the time goes in v5:
time: 44.7 us
  Pallas kernels  44 us (98%)
  between operations  0.65 us (1%)
    pallas_call x1, Pallas kernels, shards(): pl.pallas_call(kernel, out_shape=(pltpu.VMEM((ROWS, HALF), BF16), pltpu.V...  43.4 us

profile of v5, /device:TPU:1, one launch (start us, length us, event | category | flops | bytes accessed | tf_op | source)
XLA Modules:
  0.0 44.7 jit_solution(6672942219425060491)
XLA Ops:
  0.6 43.4 %shard_map.211 = (bf16[16,1024]{1,0:T(8,128)(2,1)S(1)}, bf16[16,64]{1,0:T(8,128)(2,1)S(1)}, bf16[16,64]{1,0:T(8,128)(2,1)S(1)}) custom-call(bf16[16,2048]{1,0:T(8,128)(2,1)} %tokens_h.1, s32[16]{0:T(128)} %lengths_h.1, f32[1,2048]{1,0:T(1,128)} %bitcast.19, bf16[2048,512]{1,0:T(8,128)(2,1)} %wq_h.1, bf16[64,2048]{1,0:T(8,128)(2,1)} %bitcast.17, ...), custom_call_target="tpu_custom_call" | custom-call | tf_op jit(solution)/shard_map/pallas_call | solution.py:460
  44.0 0.6 %shard_map.212 = (bf16[16,1024]{1,0:T(8,128)(2,1)}, bf16[16,64]{1,0:T(8,128)(2,1)}, bf16[16,64]{1,0:T(8,128)(2,1)}) custom-call(bf16[16,1024]{1,0:T(8,128)(2,1)S(1)} %get-tuple-element.6.refs_0_, bf16[16,64]{1,0:T(8,128)(2,1)S(1)} %get-tuple-element.7.refs_1_, bf16[16,64]{1,0:T(8,128)(2,1)S(1)} %get-tuple-element.8.refs_2_), custom_call_target="tpu_custom_call" | custom-call | tf_op jit(solution)/shard_map/pallas_call | solution.py:477

commit v6 on v5

--- a/solution.py
+++ b/solution.py
@@ -307,10 +307,6 @@
             for copy in first_hop:
                 copy.start()
 
-    stage("plane_hop")
-    settle(w3.at[:, pl.ds(0, 3), 0], w3a_r.at[0])
-    for copy in second_hop:
-        copy.start()
     xf = []
     gate_rows = [jnp.zeros((256, 256), F32)] * 2
     up_rows = [jnp.zeros((256, 256), F32)] * 2
@@ -325,6 +321,11 @@
         if c == 0:
             shared[0].wait_recv()
             shared[1].wait_recv()
+        if c == 1:
+            stage("plane_hop")
+            settle(w3.at[:, pl.ds(0, 3), 0], w3a_r.at[0])
+            for copy in second_hop:
+                copy.start()
         stage("expert_own")
         mine, part_w = rows_of(xin.at[t, c]), pl.ds(c * WIDE, WIDE)
         for k in range(2):

time: 44.7 us -> 44.7 us (level)
  no operation moved by 1% of the time
where the time goes in v6:
time: 44.7 us
  Pallas kernels  44 us (98%)
  between operations  0.65 us (1%)
    pallas_call x1, Pallas kernels, shards(): pl.pallas_call(kernel, out_shape=(pltpu.VMEM((ROWS, HALF), BF16), pltpu.V...  43.4 us

profile of v6, /device:TPU:1, one launch (start us, length us, event | category | flops | bytes accessed | tf_op | source)
XLA Modules:
  0.0 44.7 jit_solution(15461540731181748970)
XLA Ops:
  0.6 43.4 %shard_map.211 = (bf16[16,1024]{1,0:T(8,128)(2,1)S(1)}, bf16[16,64]{1,0:T(8,128)(2,1)S(1)}, bf16[16,64]{1,0:T(8,128)(2,1)S(1)}) custom-call(bf16[16,2048]{1,0:T(8,128)(2,1)} %tokens_h.1, s32[16]{0:T(128)} %lengths_h.1, f32[1,2048]{1,0:T(1,128)} %bitcast.19, bf16[2048,512]{1,0:T(8,128)(2,1)} %wq_h.1, bf16[64,2048]{1,0:T(8,128)(2,1)} %bitcast.17, ...), custom_call_target="tpu_custom_call" | custom-call | tf_op jit(solution)/shard_map/pallas_call | solution.py:461
  44.0 0.6 %shard_map.212 = (bf16[16,1024]{1,0:T(8,128)(2,1)}, bf16[16,64]{1,0:T(8,128)(2,1)}, bf16[16,64]{1,0:T(8,128)(2,1)}) custom-call(bf16[16,1024]{1,0:T(8,128)(2,1)S(1)} %get-tuple-element.6.refs_0_, bf16[16,64]{1,0:T(8,128)(2,1)S(1)} %get-tuple-element.7.refs_1_, bf16[16,64]{1,0:T(8,128)(2,1)S(1)} %get-tuple-element.8.refs_2_), custom_call_target="tpu_custom_call" | custom-call | tf_op jit(solution)/shard_map/pallas_call | solution.py:478
